TPU v7x, 128 devices: a whole 4x4x4 slice. The times are simulated.
128 devices in a mesh: sp: 16 (over z, y), dp: 8 (over x, core).
Axes of the slice: x: 4, y: 4, z: 4, core: 2. Of those that a mesh axis runs over, the one named last changes fastest.
Arguments:
- queries: bfloat16 [8, 2048, 2048], P('dp', 'sp'), may hold values from -40 to 40
- keys: bfloat16 [8, 2048, 512], P('dp', 'sp'), may hold values from -8 to 8
- values: bfloat16 [8, 2048, 512], P('dp', 'sp'), may hold values from -6 to 6
- lambdas: float32 [16], replicated, may hold values from 0.3 to 0.8
- value_gain: float32 [128], replicated, may hold values from 0.1 to 1.9
- out_weight: bfloat16 [2048, 4096], P(None, ('sp', 'dp')), may hold values from -0.125 to 0.125
Outputs:
- mixed: bfloat16 [8, 2048, 4096], P('dp', 'sp')
All inputs are finite; a program needn't handle non-finite values.
Results may differ from a plain program's by a relative error of at most 0.0087.
Values may be sent and summed in bfloat16 or wider, within the bound.
No kernel may reach another device: no remote copies, remote signals or barrier semaphores. Data moves between devices by JAX's collectives and lax.ppermute only.
A program may use at most 128 MiB of HBM per device.

v0:
```python
import jax
import jax.numpy as jnp
from jax import lax
from jax.sharding import PartitionSpec as P

HEADS = 16
KV_HEADS = 4
HEAD_DIM = 64
VALUE_DIM = 128


rope_base = 500000.0
output_scale = 0.8
norm_eps = 1e-05


def rotate(parts, positions):
    width = parts.shape[-1]
    half = width // 2
    freqs = rope_base ** (-jnp.arange(0, width, 2, dtype=jnp.float32) / width)
    angles = positions[:, None] * freqs[None, :]
    shape = (angles.shape[0],) + (1,) * (parts.ndim - 2) + (half,)
    cosine = jnp.cos(angles).reshape(shape)
    sine = jnp.sin(angles).reshape(shape)
    first = parts[..., :half]
    second = parts[..., half:]
    return jnp.concatenate([first * cosine - second * sine, second * cosine + first * sine], -1)


def attend(query_rot, key_rot, value_whole, lambda_heads, value_gain):
    seqlen = key_rot.shape[0]
    block_rows = min(512, seqlen)
    count = seqlen // block_rows
    score_scale = query_rot.shape[-1] ** (-0.5)
    outputs = []
    for block_index in range(count):
        start = block_index * block_rows
        reach = start + block_rows
        query_block = query_rot[start:reach]
        key_part = key_rot[:reach]
        value_part = value_whole[:reach]
        scores = (
            jnp.einsum("qhmd,kmd->hmqk", query_block, key_part, preferred_element_type=jnp.float32)
            * score_scale
        )
        allowed = jnp.arange(reach)[None, :] <= (start + jnp.arange(block_rows))[:, None]
        scores = jnp.where(allowed[None, None], scores, -jnp.inf)
        row_top = jnp.max(scores, -1, keepdims=True)
        raised = jnp.exp(scores - row_top)
        maps = raised / jnp.sum(raised, -1, keepdims=True)
        weights = (maps[:, 0] - lambda_heads[:, None, None] * maps[:, 1]).astype(jnp.bfloat16)
        outputs.append(
            jnp.einsum("hqk,ke->qhe", weights, value_part, preferred_element_type=jnp.float32)
        )
    head_values = jnp.concatenate(outputs, 0)
    squares = jnp.mean(head_values * head_values, -1, keepdims=True)
    normed = head_values * lax.rsqrt(squares + norm_eps) * value_gain * output_scale
    return normed.astype(jnp.bfloat16)


def shards(queries, keys, values, lambdas, value_gain, out_weight):
    tok_rows = queries.shape[1]
    sp_count = lax.axis_size("sp")
    group_size = sp_count // KV_HEADS
    per_device = HEADS // sp_count
    query_split = queries[0].reshape(tok_rows, HEADS, 2 * HEAD_DIM)
    key_split = keys[0].reshape(tok_rows, KV_HEADS, 2 * HEAD_DIM)
    value_split = values[0].reshape(tok_rows, KV_HEADS, VALUE_DIM)
    key_copies = jnp.repeat(key_split, group_size, axis=1)
    value_copies = jnp.repeat(value_split, group_size, axis=1)
    query_heads, key_heads, value_heads = (
        lax.all_to_all(query_split, "sp", split_axis=1, concat_axis=0, tiled=True),
        lax.all_to_all(key_copies, "sp", split_axis=1, concat_axis=0, tiled=True),
        lax.all_to_all(value_copies, "sp", split_axis=1, concat_axis=0, tiled=True),
    )
    key_whole = key_heads[:, 0]
    value_whole = value_heads[:, 0]
    seqlen = query_heads.shape[0]
    positions = jnp.arange(seqlen, dtype=jnp.float32)
    query_rot = rotate(
        query_heads.reshape(seqlen, per_device, 2, HEAD_DIM).astype(jnp.float32), positions
    ).astype(jnp.bfloat16)
    key_rot = rotate(key_whole.reshape(seqlen, 2, HEAD_DIM).astype(jnp.float32), positions).astype(
        jnp.bfloat16
    )
    lambda_heads = lax.dynamic_slice_in_dim(
        lambdas, lax.axis_index("sp") * per_device, per_device, 0
    )
    head_out = attend(query_rot, key_rot, value_whole, lambda_heads, value_gain)
    heads_local = lax.all_to_all(
        head_out.reshape(seqlen, per_device * VALUE_DIM),
        "sp",
        split_axis=0,
        concat_axis=1,
        tiled=True,
    )
    mixed = jnp.dot(
        heads_local,
        lax.all_gather(out_weight, ("sp", "dp"), axis=1, tiled=True),
        preferred_element_type=jnp.float32,
    ).astype(jnp.bfloat16)
    return mixed[None]


def solution(mesh):
    return jax.shard_map(
        shards,
        mesh=mesh,
        in_specs=(
            P("dp", "sp", None),
            P("dp", "sp", None),
            P("dp", "sp", None),
            P(),
            P(),
            P(None, ("sp", "dp")),
        ),
        out_specs=P("dp", "sp", None),
        check_vma=False,
    )
```

profile of v0, /device:TPU:2, one launch (start us, length us, event | category | flops | bytes accessed | tf_op | source)
XLA Modules:
  0.0 124.7 jit_solution(13890816963404634204)
XLA Ops:
  6.5 0.0 copy-start.4
  6.5 0.0 all-gather.2.cloned.1.call-start
  6.5 0.7 all-gather.2.cloned.1.call-update
  7.3 1.0 copy.19
  8.3 0.9 broadcast_in_dim.51
  9.2 8.0 %all-to-all-start = ((bf16[128,16,128]{0,2,1:T(8,128)(2,1)}), bf16[128,16,128]{0,2,1:T(8,128)(2,1)S(1)}, u32[]{:S(2)}, u32[]{:S(2)}) async-start(bf16[128,16,128]{0,2,1:T(8,128)(2,1)} %bitcast.1), calls=%async_computation | async-start | bytes 1048576 | tf_op jit(solution)/shard_map/all_to_all | solution.py:73
  17.3 0.8 iota_compare_fusion.3
  18.0 1.8 %fusion.42 = (f32[2048,32]{0,1:T(8,128)}, f32[2048,32]{0,1:T(8,128)}) fusion(f32[32]{0:T(128)S(1)} %multiply_power_fusion), kind=kLoop, calls=%fused_computation.74 | loop fusion | flops 65536 | bytes 524416 | tf_op jit(solution)/shard_map/cos | solution.py:23
  19.9 0.9 reshape_squeeze.12
  20.8 0.6 iota_compare_fusion.1
  21.4 7.4 %all-to-all-done = bf16[128,16,128]{0,2,1:T(8,128)(2,1)S(1)} async-done(((bf16[128,16,128]{0,2,1:T(8,128)(2,1)}), bf16[128,16,128]{0,2,1:T(8,128)(2,1)S(1)}, u32[]{:S(2)}, u32[]{:S(2)}) %all-to-all-start) | async-done | bytes 524320 | tf_op jit(solution)/shard_map/all_to_all | solution.py:73
  28.8 0.9 broadcast_in_dim.53
  29.7 3.6 %all-to-all-start.2 = ((bf16[128,16,128]{2,0,1:T(8,128)(2,1)}), bf16[128,16,128]{2,0,1:T(8,128)(2,1)S(1)}, u32[]{:S(2)}, u32[]{:S(2)}) async-start(bf16[128,16,128]{2,0,1:T(8,128)(2,1)} %bitcast.12), calls=%async_computation.2 | async-start | bytes 1048576 | tf_op jit(solution)/shard_map/all_to_all | solution.py:74
  33.3 0.0 copy-done.4
  33.3 1.0 copy.15
  34.3 0.0 copy-done.8
  34.3 0.6 dynamic_slice.3
  34.9 0.8 iota_compare_fusion
  35.7 8.0 %all-to-all-done.2 = bf16[128,16,128]{2,0,1:T(8,128)(2,1)S(1)} async-done(((bf16[128,16,128]{2,0,1:T(8,128)(2,1)}), bf16[128,16,128]{2,0,1:T(8,128)(2,1)S(1)}, u32[]{:S(2)}, u32[]{:S(2)}) %all-to-all-start.2) | async-done | bytes 524320 | tf_op jit(solution)/shard_map/all_to_all | solution.py:74
  43.7 4.4 %all-to-all-start.1 = ((bf16[128,16,128]{0,2,1:T(8,128)(2,1)}), bf16[128,16,128]{0,2,1:T(8,128)(2,1)}, u32[]{:S(2)}, u32[]{:S(2)}) async-start(bf16[128,16,128]{0,2,1:T(8,128)(2,1)} %bitcast.4), calls=%async_computation.1 | async-start | bytes 1048576 | tf_op jit(solution)/shard_map/all_to_all | solution.py:72
  48.1 0.4 iota_compare_fusion.2
  48.5 0.7 slice.115
  49.2 0.8 slice.122
  50.0 0.1 convert_bitcast_fusion.1
  50.1 0.0 copy-done
  50.1 1.6 %copy.14 = f32[16,128,1,128]{1,0,3,2:T(8,128)} copy(f32[16,128,1,128]{1,3,0,2:T(8,128)S(1)} %convert_bitcast_fusion.1) | data formatting | bytes 2097152 | tf_op jit(solution)/shard_map/convert_element_type | solution.py:83
  51.7 1.4 %reshape.478 = f32[2048,2,64]{0,2,1:T(8,128)S(1)} reshape(f32[16,128,1,128]{1,0,3,2:T(8,128)} %copy.14) | data formatting | bytes 2097152 | tf_op jit(solution)/shard_map/convert_element_type | solution.py:83
  53.1 8.3 %all-to-all-done.1 = bf16[128,16,128]{0,2,1:T(8,128)(2,1)} async-done(((bf16[128,16,128]{0,2,1:T(8,128)(2,1)}), bf16[128,16,128]{0,2,1:T(8,128)(2,1)}, u32[]{:S(2)}, u32[]{:S(2)}) %all-to-all-start.1) | async-done | bytes 524320 | tf_op jit(solution)/shard_map/all_to_all | solution.py:72
  61.5 1.1 convert_bitcast_fusion
  62.6 1.6 %copy.16 = f32[16,128,1,128]{1,0,3,2:T(8,128)} copy(f32[16,128,1,128]{1,3,0,2:T(8,128)S(1)} %convert_bitcast_fusion) | data formatting | bytes 2097152 | tf_op jit(solution)/shard_map/convert_element_type | solution.py:81
  64.2 2.4 %reshape.479 = f32[2048,1,2,64]{0,3,2,1:T(8,128)} reshape(f32[16,128,1,128]{1,0,3,2:T(8,128)} %copy.16) | data formatting | bytes 2097152 | tf_op jit(solution)/shard_map/convert_element_type | solution.py:81
  66.6 1.2 subtract_convert_fusion.1
  67.8 1.5 %subtract_convert_fusion = (bf16[2048,1,2,32]{0,3,2,1:T(8,128)(2,1)S(1)}, bf16[2048,1,2,32]{0,3,2,1:T(8,128)(2,1)S(1)}) fusion(f32[2048,1,2,64]{0,3,2,1:T(8,128)} %reshape.479, f32[2048,32]{0,1:T(8,128)} %get-tuple-element.10, f32[2048,32]{0,1:T(8,128)} %get-tuple-element.9), kind=kLoop, calls=%fused_computation.65 | loop fusion | flops 1048576 | bytes 2097152 | tf_op jit(solution)/shard_map/convert.6
  69.3 0.0 copy-done.2
  69.3 0.6 fusion.62
  69.9 0.3 fusion.20
  70.2 0.3 fusion.19
  70.5 1.0 fusion.32
  71.6 1.1 fusion.11
  72.6 1.0 fusion.10
  73.6 1.0 fusion.9
  74.6 0.0 copy-done.6
  74.6 1.2 fusion.28
  75.8 1.5 %fusion.5 = (f32[2,512]{1,0:T(2,128)S(1)}, f32[2,1536,512]{2,1,0:T(8,128)S(1)}) fusion(pred[512,1536]{0,1:T(8,128)(4,1)S(1)} %iota_compare_fusion.1, bf16[2048,1,2,32]{0,3,2,1:T(8,128)(2,1)S(1)} %get-tuple-element.5, bf16[2048,1,2,32]{0,3,2,1:T(8,128)(2,1)S(1)} %get-tuple-element.6, bf16[2048,2,32]{0,2,1:T(8,128)(2,1)S(1)} %get-tuple-element.7, ...), kind=kOutput, calls=%fused_computation.10 | convolution fusion | flops 207092736 | bytes 8130560 | tf_op jit(solution)/shard_map/qhmd,kmd->hmqk/dot_general | solution.py:43
  77.3 1.5 %fusion.4 = f32[2,512]{1,0:T(2,128)S(1)} fusion(f32[2,1536,512]{2,1,0:T(8,128)S(1)} %get-tuple-element.14, f32[2,512]{1,0:T(2,128)S(1)} %get-tuple-element.13, pred[512,1536]{0,1:T(8,128)(4,1)S(1)} %iota_compare_fusion.1), kind=kLoop, calls=%fused_computation.8 | loop fusion | flops 6290432 | bytes 7086080 | tf_op jit(solution)/shard_map/reduce_sum | solution.py:50
  78.8 1.7 %fusion.3 = f32[1,2,512,1536]{2,3,1,0:T(8,128)S(1)} fusion(f32[2,1536,512]{2,1,0:T(8,128)S(1)} %get-tuple-element.14, f32[2,512]{1,0:T(2,128)S(1)} %fusion.4, f32[2,512]{1,0:T(2,128)S(1)} %get-tuple-element.13, pred[512,1536]{0,1:T(8,128)(4,1)S(1)} %iota_compare_fusion.1), kind=kLoop, calls=%fused_computation.7 | loop fusion | flops 6291456 | bytes 13377536 | tf_op jit(solution)/shard_map/div | solution.py:50
  80.5 0.0 copy-done.5
  80.5 1.5 %fusion.22 = f32[512,128]{1,0:T(8,128)S(1)} fusion(bf16[1536,128]{1,0:T(8,128)(2,1)S(1)} %bitcast.127, f32[1,2,512,1536]{2,3,1,0:T(8,128)S(1)} %fusion.3, f32[]{:T(128)} %bitcast.10), kind=kOutput, calls=%fused_computation.36 | convolution fusion | flops 203685888 | bytes 6946820 | tf_op jit(solution)/shard_map/hqk,ke->qhe/dot_general | solution.py:53
  82.0 1.9 %fusion.2 = (f32[2,512]{1,0:T(2,128)S(1)}, f32[2,2048,512]{2,1,0:T(8,128)S(1)}) fusion(pred[512,2048]{0,1:T(8,128)(4,1)S(1)} %iota_compare_fusion, bf16[2048,1,2,32]{0,3,2,1:T(8,128)(2,1)S(1)} %get-tuple-element.6, bf16[2048,1,2,32]{0,3,2,1:T(8,128)(2,1)S(1)} %get-tuple-element.5, bf16[2048,2,32]{0,2,1:T(8,128)(2,1)S(1)} %get-tuple-element.8, ...), kind=kOutput, calls=%fused_computation.4 | convolution fusion | flops 276036608 | bytes 10489856 | tf_op jit(solution)/shard_map/qhmd,kmd->hmqk/dot_general | solution.py:43
  83.9 2.0 %fusion.1 = f32[2,512]{1,0:T(2,128)S(1)} fusion(f32[2,2048,512]{2,1,0:T(8,128)S(1)} %get-tuple-element.12, f32[2,512]{1,0:T(2,128)S(1)} %get-tuple-element.11, pred[512,2048]{0,1:T(8,128)(4,1)S(1)} %iota_compare_fusion), kind=kLoop, calls=%fused_computation.3 | loop fusion | flops 8387584 | bytes 9445376 | tf_op jit(solution)/shard_map/reduce_sum | solution.py:50
  85.9 0.0 copy-start.1
  86.0 2.0 %fusion = f32[1,2,512,2048]{2,3,1,0:T(8,128)S(1)} fusion(f32[2,2048,512]{2,1,0:T(8,128)S(1)} %get-tuple-element.12, f32[2,512]{1,0:T(2,128)S(1)} %fusion.1, f32[2,512]{1,0:T(2,128)S(1)} %get-tuple-element.11, pred[512,2048]{0,1:T(8,128)(4,1)S(1)} %iota_compare_fusion), kind=kLoop, calls=%fused_computation.2 | loop fusion | flops 8388608 | bytes 17833984 | tf_op jit(solution)/shard_map/div | solution.py:50
  87.9 0.0 copy-done.1
  87.9 0.0 copy-start.7
  88.0 1.7 %fusion.17 = f32[512,128]{1,0:T(8,128)S(1)} fusion(bf16[2048,128]{1,0:T(8,128)(2,1)S(1)} %bitcast.119, f32[1,2,512,2048]{2,3,1,0:T(8,128)S(1)} %fusion, f32[]{:T(128)} %bitcast.10), kind=kOutput, calls=%fused_computation.32 | convolution fusion | flops 271581184 | bytes 9175044 | tf_op jit(solution)/shard_map/hqk,ke->qhe/dot_general | solution.py:53
  89.7 0.0 copy-start.3
  89.7 0.1 pad_maximum_fusion
  89.8 0.6 copy-done.3
  90.4 0.3 copy.18
  90.7 1.3 %fusion.27 = f32[2048]{0:T(1024)S(1)} fusion(f32[512,1,128]{2,0,1:T(8,128)} %bitcast.124, f32[512,1,128]{2,0,1:T(8,128)S(1)} %bitcast.123, f32[512,1,128]{2,0,1:T(8,128)S(1)} %bitcast.122, f32[512,1,128]{2,0,1:T(8,128)S(1)} %bitcast.120), kind=kLoop, calls=%fused_computation.43 | loop fusion | flops 1308672 | bytes 1056768 | tf_op jit(solution)/shard_map/reduce_sum | solution.py:56
  92.0 0.0 copy-done.7
  92.0 0.2 multiply_convert_fusion
  92.3 13.1 %all_to_all.49 = bf16[16,128,128]{1,2,0:T(8,128)(2,1)S(1)} all-to-all(bf16[16,128,128]{1,2,0:T(8,128)(2,1)S(1)} %multiply_convert_fusion), channel_id=1, replica_groups=mesh['sp'=16,'dp'=8] {'sp'}, dimensions={0} | all-to-all | bytes 1048576 | tf_op jit(solution)/shard_map/all_to_all | solution.py:90
  105.3 12.5 %fusion.6 = bf16[1,128,4096]{2,1,0:T(8,128)(2,1)} fusion(bf16[128,2048]{0,1:T(8,128)(2,1)S(1)} %bitcast.121, bf16[2048,4096]{0,1:T(8,128)(2,1)} %all-gather.2.cloned.1.call-done), kind=kOutput, calls=%fused_computation.11 | convolution fusion | flops 2148007936 | bytes 18350080 | tf_op jit(solution)/shard_map/dot_general | solution.py:97
  (13 shorter events, 0.1 us)
Async XLA Ops:
  6.5 26.8 %copy-start.4 = (bf16[1,128,2048]{2,1,0:T(8,128)(2,1)S(1)}, bf16[1,128,2048]{2,1,0:T(8,128)(2,1)}, u32[]{:S(2)}) copy-start(bf16[1,128,2048]{2,1,0:T(8,128)(2,1)} %param.6) | copy-start | bytes 1572868
  6.5 27.8 %copy-start.8 = (f32[16]{0:T(128)S(1)}, f32[16]{0:T(128)}, u32[]{:S(2)}) copy-start(f32[16]{0:T(128)} %param.9) | copy-start | bytes 196
  6.5 98.8 %all-gather.2.cloned.1.call-start = ((), (), s32[]{:S(2)}) async-start(), calls=%async_computation.4 | async-start | bytes 16908288 | tf_op jit(solution)/shard_map/all_gather | solution.py:99
  9.2 19.6 %all-to-all-start = ((bf16[128,16,128]{0,2,1:T(8,128)(2,1)}), bf16[128,16,128]{0,2,1:T(8,128)(2,1)S(1)}, u32[]{:S(2)}, u32[]{:S(2)}) async-start(bf16[128,16,128]{0,2,1:T(8,128)(2,1)} %bitcast.1), calls=%async_computation | async-start | bytes 1048576 | tf_op jit(solution)/shard_map/all_to_all | solution.py:73
  29.7 14.0 %all-to-all-start.2 = ((bf16[128,16,128]{2,0,1:T(8,128)(2,1)}), bf16[128,16,128]{2,0,1:T(8,128)(2,1)S(1)}, u32[]{:S(2)}, u32[]{:S(2)}) async-start(bf16[128,16,128]{2,0,1:T(8,128)(2,1)} %bitcast.12), calls=%async_computation.2 | async-start | bytes 1048576 | tf_op jit(solution)/shard_map/all_to_all | solution.py:74
  43.7 6.4 %copy-start = (bf16[128,16,128]{2,0,1:T(8,128)(2,1)}, bf16[128,16,128]{2,0,1:T(8,128)(2,1)S(1)}, u32[]{:S(2)}) copy-start(bf16[128,16,128]{2,0,1:T(8,128)(2,1)S(1)} %all-to-all-done.2) | copy-start | bytes 1572868
  43.7 17.8 %all-to-all-start.1 = ((bf16[128,16,128]{0,2,1:T(8,128)(2,1)}), bf16[128,16,128]{0,2,1:T(8,128)(2,1)}, u32[]{:S(2)}, u32[]{:S(2)}) async-start(bf16[128,16,128]{0,2,1:T(8,128)(2,1)} %bitcast.4), calls=%async_computation.1 | async-start | bytes 1048576 | tf_op jit(solution)/shard_map/all_to_all | solution.py:72
  66.6 2.7 %copy-start.2 = (pred[512,512]{0,1:T(8,128)(4,1)S(1)}, pred[512,512]{0,1:T(8,128)(4,1)}, u32[]{:S(2)}) copy-start(pred[512,512]{0,1:T(8,128)(4,1)} %iota_compare_fusion.3) | copy-start | bytes 786436
  73.6 1.0 copy-start.6
  78.8 1.7 %copy-start.5 = (bf16[12,128,1,128]{3,1,0,2:T(8,128)(2,1)S(1)}, bf16[12,128,1,128]{3,1,0,2:T(8,128)(2,1)}, u32[]{:S(2)}) copy-start(bf16[12,128,1,128]{3,1,0,2:T(8,128)(2,1)} %slice.122) | copy-start | bytes 1179652
  85.9 2.0 %copy-start.1 = (bf16[128,16,128]{2,0,1:T(8,128)(2,1)S(1)}, bf16[128,16,128]{2,0,1:T(8,128)(2,1)}, u32[]{:S(2)}) copy-start(bf16[128,16,128]{2,0,1:T(8,128)(2,1)} %copy-done) | copy-start | bytes 1572868
  87.9 4.1 %copy-start.7 = (f32[128]{0:T(128)S(1)}, f32[128]{0:T(128)}, u32[]{:S(2)}) copy-start(f32[128]{0:T(128)} %param.10) | copy-start | bytes 1540
  89.7 0.7 copy-start.3
Sparse Core Ops, SparseCore 0:
  10.5 86.9 all-gather.1
where the time goes:
time: 125 us
  waiting for transfers between devices  24.4 us (20%)
  matrix products  23 us (18%)
  other arithmetic  19.6 us (16%)
  starting transfers between devices  16 us (13%)
  local copies, waits for them, and re-layouts  14.8 us (12%)
  between operations  13.7 us (11%)
  blocking collectives  13.1 us (10%)
    all_to_all x1, blocking collectives, shards(): lax.all_to_all(head_out.reshape(seqlen, per_device * VALUE_DIM), 'sp', sp...  13.1 us
    dot_general x1, matrix products, shards(): jnp.dot(heads_local, lax.all_gather(out_weight, ('sp', 'dp'), axis=1, til...  12.5 us
    all_to_all x1, waiting for transfers between devices, shards(): lax.all_to_all(query_split, 'sp', split_axis=1, concat_axis=0, tiled=True)  8.35 us
    all_to_all x1, starting transfers between devices, shards(): lax.all_to_all(key_copies, 'sp', split_axis=1, concat_axis=0, tiled=True)  8.05 us
    all_to_all x1, waiting for transfers between devices, shards(): lax.all_to_all(value_copies, 'sp', split_axis=1, concat_axis=0, tiled=True)  7.97 us
    all_to_all x1, waiting for transfers between devices, shards(): lax.all_to_all(key_copies, 'sp', split_axis=1, concat_axis=0, tiled=True)  7.36 us
    dot_general x4, matrix products, attend(): jnp.einsum('hqk,ke->qhe', weights, value_part, preferred_element_type=jnp...  5.45 us
    dot_general x4, matrix products, attend(): jnp.einsum('qhmd,kmd->hmqk', query_block, key_part, preferred_element_typ...  5.07 us
  transfers between devices with their start and end apart: 4, of which 3 were waited for; matrix products, arithmetic and copies ran while one was open for 36% of the time, Pallas kernels for 0%

commit v1 on v0

v1 whole, which is shorter than its diff:
```python
import functools

import jax
import jax.numpy as jnp
from jax import lax
from jax.experimental import pallas as pl
from jax.experimental.pallas import tpu as pltpu
from jax.sharding import Mesh
from jax.sharding import PartitionSpec as P


F32 = jnp.float32
BF16 = jnp.bfloat16
HEAD_DIM = 64
ROPE_BASE = 500000.0
OUTPUT_SCALE = 0.8
NORM_EPS = 1e-05
BLOCK = 128
SEQ = 2048
PARTS = 2

VM = pl.BlockSpec(memory_space=pltpu.VMEM)
SM = pl.BlockSpec(memory_space=pltpu.SMEM)


def cost(flops, size):
    return pl.CostEstimate(flops=flops, bytes_accessed=size, transcendentals=0)


def room(mib):
    return pltpu.CompilerParams(vmem_limit_bytes=mib * 1024 * 1024)


def shape(*dims):
    return jax.ShapeDtypeStruct(dims, BF16)


def hop(axis, step, x):
    return lax.ppermute(x, axis, [(i, (i + step) % 4) for i in range(4)])


def line(axis, x):
    return x, hop(axis, 1, x), hop(axis, 3, x), hop(axis, 2, x)


ORDER = (0, 3, 1, 2)


def rotate_kernel(lambdas, gain_ref, q_ref, k_ref, v_ref, w_ref, cos_ref, sin_ref, kv_out, w_out, const_out, *q_out):
    z = lax.axis_index("z")
    const_out[:1] = gain_ref[...]
    for h in range(4):
        const_out[h + 1 : h + 2] = jnp.full((1, 128), lambdas[z * 4 + h], F32)
    const_out[5:] = jnp.zeros((3, 128), F32)
    w_out[...] = w_ref[...]
    cosine = cos_ref[...]
    sine = sin_ref[...]
    lane = lax.broadcasted_iota(jnp.int32, (BLOCK, 128), 1)
    low = (lane % HEAD_DIM) < HEAD_DIM // 2

    def turn(x):
        x = x.astype(F32)
        other = jnp.where(low, pltpu.roll(x, 96, 1), pltpu.roll(x, 32, 1))
        return (x * cosine + other * sine).astype(BF16)

    for g in range(4):
        kv_out[g, :, :128] = turn(k_ref[0, :, g * 128 : (g + 1) * 128])
        kv_out[g, :, 128:] = v_ref[0, :, g * 128 : (g + 1) * 128]
    for r in range(4):
        group = lax.rem(z + r, 4) * 512
        for h in range(4):
            at = pl.multiple_of(group + h * 128, 128)
            q_out[r][:, h * 128 : (h + 1) * 128] = turn(q_ref[0, :, pl.ds(at, 128)]) * BF16(0.125)


def rotate(lambdas, gain, q, k, v, w, cosine, sine):
    return pl.pallas_call(
        rotate_kernel,
        in_specs=[SM] + [VM] * 7,
        out_specs=[VM] * 7,
        out_shape=[shape(4, BLOCK, 256), shape(*w.shape), jax.ShapeDtypeStruct((8, 128), F32)]
        + [shape(BLOCK, 512)] * 4,
        cost_estimate=cost(2**20, 2**20),
        compiler_params=room(8),
        name="rotate",
    )(lambdas, gain, q, k, v, w, cosine, sine)


def attend_kernel(rows, const, *refs):
    z = lax.axis_index("z")
    y = lax.axis_index("y")
    gain = const[:1]
    q_refs, refs = refs[:4], refs[4:]
    if len(refs) == 8:
        kv_refs, (out_ref, kbuf, vbuf, q_ref) = refs[:4], refs[4:]
        for r, ref in enumerate(kv_refs):
            src = lax.rem(y + ORDER[r], 4)
            for j in range(4):
                at = pl.multiple_of(j * 512 + src * 128, 128)
                kbuf[:, pl.ds(at, 128)] = ref[j, :, :128].T
                vbuf[pl.ds(at, 128), :] = ref[j, :, 128:]
    else:
        kbuf, vbuf, out_ref, q_ref = refs
    for r, ref in enumerate(q_refs):
        q_ref[lax.rem(z + 4 - r, 4)] = ref[rows, :]
    count = rows.stop - rows.start
    heads = BLOCK // count
    first = lax.broadcasted_iota(jnp.int32, (count, 128), 1) < HEAD_DIM
    zero = jnp.zeros((count, 128), BF16)
    key_at = lax.broadcasted_iota(jnp.int32, (2 * BLOCK, 512), 1)
    query_at = lax.broadcasted_iota(jnp.int32, (2 * BLOCK, 512), 0) % count + rows.start
    allowed = key_at <= query_at + y * BLOCK
    row_head = lax.broadcasted_iota(jnp.int32, (BLOCK, 1), 0) // count

    for i in range(4):
        reach = (i + 1) * 512
        for g in range(4 // heads):
            qs = [q_ref[i, :, h * 128 : (h + 1) * 128] for h in range(g * heads, (g + 1) * heads)]
            q = jnp.concatenate([jnp.where(first, q, zero) for q in qs] + [jnp.where(first, zero, q) for q in qs], 0)
            last = jnp.dot(q, kbuf[:, reach - 512 : reach], preferred_element_type=F32)
            last = jnp.where(allowed, last, -jnp.inf)
            top = jnp.max(last, 1, keepdims=True)
            if i:
                rest = jnp.dot(q, kbuf[:, : reach - 512], preferred_element_type=F32)
                top = jnp.maximum(top, jnp.max(rest, 1, keepdims=True))
                rest = jnp.exp(rest - top)
            last = jnp.exp(last - top)
            total = jnp.sum(last, 1, keepdims=True)
            if i:
                total = total + jnp.sum(rest, 1, keepdims=True)
            scale = 1.0 / total
            one = scale[:BLOCK]
            factor = const[g * heads + 1 : g * heads + 2, :1]
            if heads == 2:
                factor = jnp.where(row_head == 0, factor, const[g * heads + 2 : g * heads + 3, :1])
            two = scale[BLOCK:] * factor
            w = (last[:BLOCK] * one - last[BLOCK:] * two).astype(BF16)
            acc = jnp.dot(w, vbuf[reach - 512 : reach], preferred_element_type=F32)
            if i:
                w = (rest[:BLOCK] * one - rest[BLOCK:] * two).astype(BF16)
                acc = acc + jnp.dot(w, vbuf[: reach - 512], preferred_element_type=F32)
            square = jnp.mean(acc * acc, 1, keepdims=True)
            acc = acc * (lax.rsqrt(square + NORM_EPS) * OUTPUT_SCALE) * gain
            acc = acc.astype(BF16)
            for k in range(heads):
                h = g * heads + k
                out_ref[i * count : (i + 1) * count, h * 128 : (h + 1) * 128] = acc[k * count : (k + 1) * count]


def attend(rows, const, q, keys):
    count = rows.stop - rows.start
    outs = [shape(4 * count, 512)]
    if len(keys) == 4:
        outs += [shape(128, SEQ), shape(SEQ, 128)]
    return pl.pallas_call(
        functools.partial(attend_kernel, rows),
        in_specs=[VM] * (5 + len(keys)),
        out_specs=[VM] * len(outs),
        out_shape=outs,
        scratch_shapes=[pltpu.VMEM((4, count, 512), BF16)],
        compiler_params=room(16),
        cost_estimate=cost(2**31, 2**22),
        name="attend",
    )(const, *q, *keys)


ANY = pl.BlockSpec(memory_space=pl.ANY)


def stack_kernel(_, *refs):
    out = refs[-1]
    at = 0
    for ref in refs[:-1]:
        out[at : at + ref.shape[0]] = ref[...]
        at += ref.shape[0]


def stack(after, parts):
    rows = sum(p.shape[0] for p in parts)
    return pl.pallas_call(
        stack_kernel,
        in_specs=[ANY] + [VM] * len(parts),
        out_specs=VM,
        out_shape=shape(rows, parts[0].shape[1]),
        cost_estimate=cost(2**20, 2**20),
        compiler_params=room(4),
        name="stack",
    )(after, *parts)


def columns_kernel(*refs):
    y, x, c = (lax.axis_index(a) for a in "yxc")
    wbuf = refs[-1]
    for k in range(2):
        side = c if k == 0 else 1 - c
        for a in range(4):
            ax = lax.rem(x + ORDER[a], 4)
            for b in range(4):
                by = lax.rem(y + ORDER[b], 4)
                at = pl.multiple_of(by * 256 + ax * 64 + side * 32, 32)
                wbuf[pl.ds(at, 32), :] = refs[4 * k + a][b * 32 : (b + 1) * 32, :]


def columns(parts):
    return pl.pallas_call(
        columns_kernel,
        in_specs=[VM] * 8,
        out_specs=VM,
        out_shape=shape(1024, 2048),
        compiler_params=room(12),
        cost_estimate=cost(2**29, 2**23),
        name="columns",
    )(*parts)


def project_kernel(_, x0, x1, x2, x3, wbuf, *refs):
    outs, xbuf = refs[:4], refs[4]
    z = lax.axis_index("z")
    count = x0.shape[0] // 4
    for r, ref in enumerate((x0, x1, x2, x3)):
        at = pl.multiple_of(lax.rem(z + ORDER[r], 4) * 512, 512)
        xbuf[:, pl.ds(at, 512)] = ref[...]
    for n in range(4):
        cols = slice(n * 256, (n + 1) * 256)
        part = lax.dot_general(
            xbuf[...], wbuf[cols, :], (((1,), (1,)), ((), ())), preferred_element_type=F32
        ).astype(BF16)
        for i in range(4):
            for r in range(4):

                @pl.when(lax.rem(i + 4 - z, 4) == r)
                def _():
                    outs[r][:, cols] = part[i * count : (i + 1) * count]


def project(after, xs, weights):
    rows = xs[0].shape[0]
    return pl.pallas_call(
        project_kernel,
        in_specs=[ANY] + [VM] * 5,
        out_specs=[VM] * 4,
        out_shape=[shape(rows // 4, 1024)] * 4,
        scratch_shapes=[pltpu.VMEM((rows, 2048), BF16)],
        compiler_params=room(16),
        cost_estimate=cost(2**30, 2**22),
        name="project",
    )(after, *xs, weights)


def join_kernel(*refs):
    z = lax.axis_index("z")
    for r in range(4):
        at = pl.multiple_of(lax.rem(z + 4 - r, 4) * 1024, 1024)
        refs[-1][0, :, pl.ds(at, 1024)] = refs[r][...]


def join(p, pieces, whole):
    count = pieces[0].shape[0]
    return pl.pallas_call(
        join_kernel,
        grid=(1,),
        in_specs=[pl.BlockSpec((count, 1024), lambda i: (0, 0))] * 4 + ([] if whole is None else [ANY]),
        out_specs=pl.BlockSpec((1, count, 4096), lambda i: (0, p, 0)),
        out_shape=shape(1, BLOCK, 4096),
        input_output_aliases={} if whole is None else {4: 0},
        cost_estimate=cost(2**18, 2**21),
        compiler_params=room(6),
        name="join",
    )(*pieces, *(() if whole is None else (whole,)))


def shards(queries, keys, values, lambdas, value_gain, out_weight):
    first = ((lax.axis_index("z") * 4 + lax.axis_index("y")) * BLOCK).astype(jnp.int32)
    positions = (first + jnp.arange(BLOCK)).astype(F32)
    freqs = ROPE_BASE ** (-jnp.arange(0, HEAD_DIM, 2, dtype=F32) / HEAD_DIM)
    angles = positions[:, None] * jnp.tile(freqs, 4)[None, :]
    cosine = jnp.cos(angles)
    sign = jnp.where(jnp.arange(128) % HEAD_DIM < HEAD_DIM // 2, -1.0, 1.0).astype(F32)
    sine = jnp.sin(angles) * sign[None, :]
    gain = value_gain.reshape(1, 128)
    kv_split, wt, const, *q_split = rotate(lambdas, gain, queries, keys, values, out_weight.T, cosine, sine)

    kv_line = lax.all_to_all(kv_split, "z", 0, 0)
    kv_all = line("y", kv_line)
    q = [q_split[0]] + [hop("z", r, q_split[r]) for r in (1, 2, 3)]

    wy = line("y", wt)
    wy = stack(kv_line, wy)
    wx = line("x", wy)
    wc = tuple(lax.ppermute(p, "c", [(0, 1), (1, 0)]) for p in wx)
    weights = columns(wx + wc)

    count = BLOCK // PARTS
    keys_all = kv_all
    heads = []
    for p in range(PARTS):
        got, *whole = attend(slice(p * count, (p + 1) * count), const, q, keys_all)
        keys_all = whole or keys_all
        heads.append(got)
    out = None
    for p in range(PARTS):
        got = line("z", heads[p])
        sent = project(heads[-1], got, weights)
        got = [sent[0]] + [hop("z", r, sent[r]) for r in (1, 2, 3)]
        out = join(p, got, out)
    return out


def solution(mesh):
    fine = Mesh(mesh.devices.reshape(4, 4, 4, 2), ("z", "y", "x", "c"))
    tokens = P(("x", "c"), ("z", "y"), None)
    return jax.shard_map(
        shards,
        mesh=fine,
        in_specs=(tokens, tokens, tokens, P(), P(), P(None, ("z", "y", "x", "c"))),
        out_specs=tokens,
        check_vma=False,
    )
```

time: 125 us -> 109 us (0.87)
  starting transfers between devices: 16 us -> 43.2 us
  matrix products: 23 us -> 0 us
  Pallas kernels: 0 us -> 22.7 us
  other arithmetic: 19.6 us -> 0.33 us
  between operations: 13.7 us -> 0.17 us
  blocking collectives: 13.1 us -> 0 us
  waiting for transfers between devices: 24.4 us -> 36.2 us
  local copies, waits for them, and re-layouts: 14.8 us -> 5.14 us
    ppermute x0 -> x28, starting transfers between devices: none -> 37.9 us  [the longest x24 37.3 us: hop(): return lax.ppermute(x, axis, [(i, (i + step) % 4) for i in range(4)])]
    ppermute x0 -> x28, waiting for transfers between devices: none -> 36.2 us  [the longest x24 36.2 us: hop(): return lax.ppermute(x, axis, [(i, (i + step) % 4) for i in range(4)])]
    all_to_all x3 -> x1, waiting for transfers between devices: 23.7 us -> 0.01 us  [shards(): kv_line = lax.all_to_all(kv_split, 'z', 0, 0)]
    dot_general x9 -> x0, matrix products: 23 us -> none  [the longest x1 12.5 us: shards(): jnp.dot(heads_local, lax.all_gather(out_weight, ('sp', 'dp'), axis=1, til...]
    pallas_call x0 -> x9, Pallas kernels: none -> 22.7 us  [the longest x2 12.6 us: attend(): pl.pallas_call(functools.partial(attend_kernel, rows), in_specs=[VM] * (5...]
    all_to_all x1 -> x0, blocking collectives: 13.1 us -> none  [shards(): lax.all_to_all(head_out.reshape(seqlen, per_device * VALUE_DIM), 'sp', sp...]
    all_to_all x3 -> x1, starting transfers between devices: 16 us -> 5.31 us  [shards(): kv_line = lax.all_to_all(kv_split, 'z', 0, 0)]
    convert_element_type x4 -> x0, local copies, waits for them, and re-layouts: 6.96 us -> none  [the longest x2 3.96 us: shards(): query_heads.reshape(seqlen, per_device, 2, HEAD_DIM).astype(jnp.float32)]
  transfers between devices with their start and end apart: 4 -> 29, of which waited for: 3 -> 11; matrix products, arithmetic and copies ran while one was open for 36% -> 0% of each run, Pallas kernels for 0% -> 19%
where the time goes in v1:
time: 109 us; the launch traced here: 108 us
  starting transfers between devices  43.2 us (40%)
  waiting for transfers between devices  36.2 us (33%)
  Pallas kernels  22.7 us (21%)
  local copies, waits for them, and re-layouts  5.14 us (5%)
    ppermute x24, starting transfers between devices, hop(): return lax.ppermute(x, axis, [(i, (i + step) % 4) for i in range(4)])  37.3 us
    ppermute x24, waiting for transfers between devices, hop(): return lax.ppermute(x, axis, [(i, (i + step) % 4) for i in range(4)])  36.2 us
    pallas_call x2, Pallas kernels, attend(): pl.pallas_call(functools.partial(attend_kernel, rows), in_specs=[VM] * (5...  12.6 us
    pallas_call x2, Pallas kernels, project(): pl.pallas_call(project_kernel, in_specs=[ANY] + [VM] * 5, out_specs=[VM]...  6.3 us
    all_to_all x1, starting transfers between devices, shards(): kv_line = lax.all_to_all(kv_split, 'z', 0, 0)  5.31 us
    unnamed x12, local copies, waits for them, and re-layouts  5.06 us
  transfers between devices with their start and end apart: 29, of which 11 were waited for; matrix products, arithmetic and copies ran while one was open for 0% of the time, Pallas kernels for 19%

profile of v1, /device:TPU:2, one launch (start us, length us, event | category | flops | bytes accessed | tf_op | source)
XLA Modules:
  0.0 107.8 jit_solution(2896104944231722978)
XLA Ops:
  0.1 0.1 mul.44
  0.1 0.3 fusion
  0.5 0.0 copy-start
  0.5 1.0 copy-done
  1.5 0.9 copy-done.1
  2.4 0.9 copy-done.2
  3.3 0.9 copy-done.3
  4.2 0.7 copy-done.4
  4.9 0.7 copy-done.5
  5.5 1.8 %rotate.1 = (bf16[4,128,256]{2,1,0:T(8,128)(2,1)}, bf16[32,2048]{1,0:T(8,128)(2,1)S(1)}, f32[8,128]{1,0:T(8,128)S(1)}, bf16[128,512]{1,0:T(8,128)(2,1)S(1)}, bf1...) custom-call(f32[16]{0:T(128)S(1)} %copy-done.4, f32[1,128]{1,0:T(1,128)S(1)} %bitcast.3, ...), custom_call_target="tpu_custom_call" | custom-call | flops 1048576 | bytes 1048576 | tf_op jit(solution)/shard_map/rotate/pallas_call | solution.py:77
  7.3 5.3 %all-to-all-start = ((bf16[4,128,256]{2,1,0:T(8,128)(2,1)}), bf16[4,128,256]{2,1,0:T(8,128)(2,1)S(1)}, u32[]{:S(2)}, u32[]{:S(2)}) async-start(bf16[4,128,256]{2,1,0:T(8,128)(2,1)} %get-tuple-element.28), calls=%async_computation | async-start | bytes 524288 | tf_op jit(solution)/shard_map/all_to_all | solution.py:283
  12.6 3.0 %collective-permute-start.10 = (bf16[32,2048]{1,0:T(8,128)(2,1)S(1)}, bf16[32,2048]{1,0:T(8,128)(2,1)S(1)}, u32[]{:S(2)}, u32[]{:S(2)}) collective-permute-start(bf16[32,2048]{1,0:T(8,128)(2,1)S(1)} %get-tuple-element.31.refs_0_), channel_id=1, source_target_pairs={{0,24},{8,0},{16,8},{24,16},{1,25},{9,1},{17,9},{25,17},{2,26},{10... | collective-permute-start | bytes 393224 | tf_op jit(solution)/shard_map/ppermute | solution.py:39
  15.6 0.6 collective-permute-start.11
  16.2 1.0 collective-permute-start.9
  17.2 2.0 %collective-permute-start = (bf16[128,512]{1,0:T(8,128)(2,1)S(1)}, bf16[128,512]{1,0:T(8,128)(2,1)S(1)}, u32[]{:S(2)}, u32[]{:S(2)}) collective-permute-start(bf16[128,512]{1,0:T(8,128)(2,1)S(1)} %get-tuple-element.25), channel_id=1, source_target_pairs={{0,32},{32,64},{64,96},{96,0},{1,33},{33,65},{65,97},{97,1},{2,34}... | collective-permute-start | bytes 393224 | tf_op jit(solution)/shard_map/ppermute | solution.py:39
  19.2 2.7 %collective-permute-start.1 = (bf16[128,512]{1,0:T(8,128)(2,1)S(1)}, bf16[128,512]{1,0:T(8,128)(2,1)S(1)}, u32[]{:S(2)}, u32[]{:S(2)}) collective-permute-start(bf16[128,512]{1,0:T(8,128)(2,1)S(1)} %get-tuple-element.26), channel_id=1, source_target_pairs={{0,64},{32,96},{64,0},{96,32},{1,65},{33,97},{65,1},{97,33},{2,66}... | collective-permute-start | bytes 393224 | tf_op jit(solution)/shard_map/ppermute | solution.py:39
  21.9 1.3 %collective-permute-done.11.refs_3_ = bf16[32,2048]{1,0:T(8,128)(2,1)S(1)} collective-permute-done((bf16[32,2048]{1,0:T(8,128)(2,1)S(1)}, bf16[32,2048]{1,0:T(8,128)(2,1)S(1)}, u32[]{:S(2)}, u32[]{:S(2)}) %collective-permute-start.11) | collective-permute-done | bytes 131104 | tf_op jit(solution)/shard_map/ppermute | solution.py:39
  23.2 1.4 %collective-permute-done.9.refs_1_ = bf16[32,2048]{1,0:T(8,128)(2,1)S(1)} collective-permute-done((bf16[32,2048]{1,0:T(8,128)(2,1)S(1)}, bf16[32,2048]{1,0:T(8,128)(2,1)S(1)}, u32[]{:S(2)}, u32[]{:S(2)}) %collective-permute-start.9) | collective-permute-done | bytes 131104 | tf_op jit(solution)/shard_map/ppermute | solution.py:39
  24.6 0.0 all-to-all-done.refs_4_._
  24.6 1.6 %collective-permute-start.12 = (bf16[128,2048]{1,0:T(8,128)(2,1)S(1)}, bf16[128,2048]{1,0:T(8,128)(2,1)S(1)}, u32[]{:S(2)}, u32[]{:S(2)}) collective-permute-start(bf16[128,2048]{1,0:T(8,128)(2,1)S(1)} %stack.1.refs_0_), channel_id=1, source_target_pairs={{0,2},{2,4},{4,6},{6,0},{1,3},{3,5},{5,7},{7,1},{8,10},{10,12},{12... | collective-permute-start | bytes 1572872 | tf_op jit(solution)/shard_map/ppermute | solution.py:39
  26.2 0.5 collective-permute-start.13
  26.7 2.1 %collective-permute-start.14 = (bf16[128,2048]{1,0:T(8,128)(2,1)S(1)}, bf16[128,2048]{1,0:T(8,128)(2,1)S(1)}, u32[]{:S(2)}, u32[]{:S(2)}) collective-permute-start(bf16[128,2048]{1,0:T(8,128)(2,1)S(1)} %stack.1.refs_0_), channel_id=1, source_target_pairs={{0,4},{2,6},{4,0},{6,2},{1,5},{3,7},{5,1},{7,3},{8,12},{10,14},{12... | collective-permute-start | bytes 1572872 | tf_op jit(solution)/shard_map/ppermute | solution.py:39
  28.9 0.0 collective-permute-done.refs_1_
  28.9 0.0 collective-permute-start.3
  28.9 0.0 collective-permute-done.1.refs_2_
  28.9 3.0 %collective-permute-start.2 = (bf16[128,512]{1,0:T(8,128)(2,1)S(1)}, bf16[128,512]{1,0:T(8,128)(2,1)S(1)}, u32[]{:S(2)}, u32[]{:S(2)}) collective-permute-start(bf16[128,512]{1,0:T(8,128)(2,1)S(1)} %get-tuple-element.27), channel_id=1, source_target_pairs={{0,96},{32,0},{64,32},{96,64},{1,97},{33,1},{65,33},{97,65},{2,98}... | collective-permute-start | bytes 393224 | tf_op jit(solution)/shard_map/ppermute | solution.py:39
  31.9 2.5 %collective-permute-done.2.refs_3_ = bf16[128,512]{1,0:T(8,128)(2,1)S(1)} collective-permute-done((bf16[128,512]{1,0:T(8,128)(2,1)S(1)}, bf16[128,512]{1,0:T(8,128)(2,1)S(1)}, u32[]{:S(2)}, u32[]{:S(2)}) %collective-permute-start.2) | collective-permute-done | bytes 131104 | tf_op jit(solution)/shard_map/ppermute | solution.py:39
  34.4 3.2 %collective-permute-start.4 = (bf16[4,128,256]{2,1,0:T(8,128)(2,1)S(1)}, bf16[4,128,256]{2,1,0:T(8,128)(2,1)S(1)}, u32[]{:S(2)}, u32[]{:S(2)}) collective-permute-start(bf16[4,128,256]{2,1,0:T(8,128)(2,1)S(1)} %all-to-all-done.refs_4_._), channel_id=1, source_target_pairs={{0,24},{8,0},{16,8},{24,16},{1,25},{9,1},{17,9},{25,17},{2,26},{10... | collective-permute-start | bytes 786440 | tf_op jit(solution)/shard_map/ppermute | solution.py:39
  37.6 0.0 collective-permute-done.3.refs_5_
  37.6 0.0 collective-permute-start.5
  37.6 8.7 %collective-permute-done.4.refs_6_ = bf16[4,128,256]{2,1,0:T(8,128)(2,1)S(1)} collective-permute-done((bf16[4,128,256]{2,1,0:T(8,128)(2,1)S(1)}, bf16[4,128,256]{2,1,0:T(8,128)(2,1)S(1)}, u32[]{:S(2)}, u32[]{:S(2)}) %collective-permute-start.4) | collective-permute-done | bytes 262176 | tf_op jit(solution)/shard_map/ppermute | solution.py:39
  46.3 0.5 collective-permute-start.16
  46.8 0.1 collective-permute-start.17
  46.9 4.3 %collective-permute-done.14.refs_3_ = bf16[128,2048]{1,0:T(8,128)(2,1)S(1)} collective-permute-done((bf16[128,2048]{1,0:T(8,128)(2,1)S(1)}, bf16[128,2048]{1,0:T(8,128)(2,1)S(1)}, u32[]{:S(2)}, u32[]{:S(2)}) %collective-permute-start.14) | collective-permute-done | bytes 524320 | tf_op jit(solution)/shard_map/ppermute | solution.py:39
  51.3 0.0 collective-permute-start.18
  51.3 0.0 collective-permute-done.5.refs_7_
  51.3 6.4 %attend.2 = (bf16[256,512]{1,0:T(8,128)(2,1)S(1)}, bf16[128,2048]{1,0:T(8,128)(2,1)S(1)}, bf16[2048,128]{1,0:T(8,128)(2,1)S(1)}) custom-call(f32[8,128]{1,0:T(8,128)S(1)} %get-tuple-element.23.const, bf16[128,512]{1,0:T(8,128)(2,1)S(1)} %get-tuple-element.24.refs_0_, bf16[128,512]{1,0:T(8,128)(2,1)S(1)} %collective-permute-done.refs_1_, ...), custom_call_target="tpu_custom_call" | custom-call | flops 2147483648 | bytes 4194304 | tf_op jit(solution)/shard_map/attend/pallas_call | solution.py:155
  57.7 1.5 %collective-permute-start.22 = (bf16[256,512]{1,0:T(8,128)(2,1)S(1)}, bf16[256,512]{1,0:T(8,128)(2,1)S(1)}, u32[]{:S(2)}, u32[]{:S(2)}) collective-permute-start(bf16[256,512]{1,0:T(8,128)(2,1)S(1)} %get-tuple-element.36.x0), channel_id=1, source_target_pairs={{0,32},{32,64},{64,96},{96,0},{1,33},{33,65},{65,97},{97,1},{2,34}... | collective-permute-start | bytes 786440 | tf_op jit(solution)/shard_map/ppermute | solution.py:39
  59.2 0.0 collective-permute-done.15.refs_4_
  59.2 1.8 %collective-permute-start.23 = (bf16[256,512]{1,0:T(8,128)(2,1)S(1)}, bf16[256,512]{1,0:T(8,128)(2,1)S(1)}, u32[]{:S(2)}, u32[]{:S(2)}) collective-permute-start(bf16[256,512]{1,0:T(8,128)(2,1)S(1)} %get-tuple-element.36.x0), channel_id=1, source_target_pairs={{0,96},{32,0},{64,32},{96,64},{1,97},{33,1},{65,33},{97,65},{2,98}... | collective-permute-start | bytes 786440 | tf_op jit(solution)/shard_map/ppermute | solution.py:39
  61.0 6.7 %collective-permute-done.22.x1 = bf16[256,512]{1,0:T(8,128)(2,1)S(1)} collective-permute-done((bf16[256,512]{1,0:T(8,128)(2,1)S(1)}, bf16[256,512]{1,0:T(8,128)(2,1)S(1)}, u32[]{:S(2)}, u32[]{:S(2)}) %collective-permute-start.22) | collective-permute-done | bytes 262176 | tf_op jit(solution)/shard_map/ppermute | solution.py:39
  67.7 1.8 %collective-permute-start.24 = (bf16[256,512]{1,0:T(8,128)(2,1)S(1)}, bf16[256,512]{1,0:T(8,128)(2,1)S(1)}, u32[]{:S(2)}, u32[]{:S(2)}) collective-permute-start(bf16[256,512]{1,0:T(8,128)(2,1)S(1)} %get-tuple-element.36.x0), channel_id=1, source_target_pairs={{0,64},{32,96},{64,0},{96,32},{1,65},{33,97},{65,1},{97,33},{2,66}... | collective-permute-start | bytes 786440 | tf_op jit(solution)/shard_map/ppermute | solution.py:39
  69.5 6.2 %attend.3._.x0 = bf16[256,512]{1,0:T(8,128)(2,1)S(1)} custom-call(f32[8,128]{1,0:T(8,128)S(1)} %get-tuple-element.23.const, bf16[128,512]{1,0:T(8,128)(2,1)S(1)} %get-tuple-element.24.refs_0_, bf16[128,512]{1,0:T(8,128)(2,1)S(1)} %collective-permute-done.refs_1_, bf16[128,512]{1,0:T(8,128)(2,1)S(1)} %collective-permute-done.1.refs_2_, ...), custom_call_target="tpu_custom_call" | custom-call | flops 2147483648 | bytes 4194304 | tf_op jit(solution)/shard_map/attend/pallas_call | solution.py:155
  75.7 0.8 collective-permute-start.6
  76.5 2.7 %collective-permute-start.7 = (bf16[256,512]{1,0:T(8,128)(2,1)S(1)}, bf16[256,512]{1,0:T(8,128)(2,1)S(1)}, u32[]{:S(2)}, u32[]{:S(2)}) collective-permute-start(bf16[256,512]{1,0:T(8,128)(2,1)S(1)} %attend.3._.x0), channel_id=1, source_target_pairs={{0,96},{32,0},{64,32},{96,64},{1,97},{33,1},{65,33},{97,65},{2,98}... | collective-permute-start | bytes 786440 | tf_op jit(solution)/shard_map/ppermute | solution.py:39
  79.2 0.6 collective-permute-start.8
  79.8 0.3 columns.1.wbuf
  80.1 0.0 collective-permute-done.23.x2
  80.1 3.2 %project.3 = (bf16[64,1024]{1,0:T(8,128)(2,1)S(1)}, bf16[64,1024]{1,0:T(8,128)(2,1)S(1)}, bf16[64,1024]{1,0:T(8,128)(2,1)S(1)}, bf16[64,1024]{1,0:T(8,128)(2,1)S(1)}) custom-call(bf16[256,512]{1,0:T(8,128)(2,1)S(1)} %attend.3._.x0, bf16[256,512]{1,0:T(8,128)(2,1)S(1)} %get-tuple-element.36.x0, bf16[256,512]{1,0:T(8,128)(2,1)S(1)} %collective-permute-done.22.x1, ...), custom_call_target="tpu_custom_call" | custom-call | flops 1073741824 | bytes 4194304 | tf_op jit(solution)/shard_map/project/pallas_call | solution.py:238
  83.2 0.4 collective-permute-start.25
  83.7 2.7 %collective-permute-start.26 = (bf16[64,1024]{1,0:T(8,128)(2,1)S(1)}, bf16[64,1024]{1,0:T(8,128)(2,1)S(1)}, u32[]{:S(2)}, u32[]{:S(2)}) collective-permute-start(bf16[64,1024]{1,0:T(8,128)(2,1)S(1)} %get-tuple-element.39), channel_id=1, source_target_pairs={{0,64},{32,96},{64,0},{96,32},{1,65},{33,97},{65,1},{97,33},{2,66}... | collective-permute-start | bytes 393224 | tf_op jit(solution)/shard_map/ppermute | solution.py:39
  86.4 4.3 %collective-permute-done.6.x1 = bf16[256,512]{1,0:T(8,128)(2,1)S(1)} collective-permute-done((bf16[256,512]{1,0:T(8,128)(2,1)S(1)}, bf16[256,512]{1,0:T(8,128)(2,1)S(1)}, u32[]{:S(2)}, u32[]{:S(2)}) %collective-permute-start.6) | collective-permute-done | bytes 262176 | tf_op jit(solution)/shard_map/ppermute | solution.py:39
  90.7 2.8 %collective-permute-done.7.x2 = bf16[256,512]{1,0:T(8,128)(2,1)S(1)} collective-permute-done((bf16[256,512]{1,0:T(8,128)(2,1)S(1)}, bf16[256,512]{1,0:T(8,128)(2,1)S(1)}, u32[]{:S(2)}, u32[]{:S(2)}) %collective-permute-start.7) | collective-permute-done | bytes 262176 | tf_op jit(solution)/shard_map/ppermute | solution.py:39
  93.5 0.0 collective-permute-done.8.x3
  93.5 3.1 %project.2 = (bf16[64,1024]{1,0:T(8,128)(2,1)S(1)}, bf16[64,1024]{1,0:T(8,128)(2,1)S(1)}, bf16[64,1024]{1,0:T(8,128)(2,1)S(1)}, bf16[64,1024]{1,0:T(8,128)(2,1)S(1)}) custom-call(bf16[256,512]{1,0:T(8,128)(2,1)S(1)} %attend.3._.x0, bf16[256,512]{1,0:T(8,128)(2,1)S(1)} %attend.3._.x0, bf16[256,512]{1,0:T(8,128)(2,1)S(1)} %collective-permute-done.6.x1, ...), custom_call_target="tpu_custom_call" | custom-call | flops 1073741824 | bytes 4194304 | tf_op jit(solution)/shard_map/project/pallas_call | solution.py:238
  96.6 0.1 collective-permute-start.19
  96.7 5.3 %collective-permute-start.20 = (bf16[64,1024]{1,0:T(8,128)(2,1)S(1)}, bf16[64,1024]{1,0:T(8,128)(2,1)S(1)}, u32[]{:S(2)}, u32[]{:S(2)}) collective-permute-start(bf16[64,1024]{1,0:T(8,128)(2,1)S(1)} %get-tuple-element.34), channel_id=1, source_target_pairs={{0,64},{32,96},{64,0},{96,32},{1,65},{33,97},{65,1},{97,33},{2,66}... | collective-permute-start | bytes 393224 | tf_op jit(solution)/shard_map/ppermute | solution.py:39
  102.0 0.0 collective-permute-done.25.refs_1_
  102.0 0.0 collective-permute-start.21
  102.0 0.8 join.2.refs_4_
  102.8 0.6 collective-permute-done.19.refs_1_
  103.5 2.9 %collective-permute-done.20.refs_2_ = bf16[64,1024]{1,0:T(8,128)(2,1)S(1)} collective-permute-done((bf16[64,1024]{1,0:T(8,128)(2,1)S(1)}, bf16[64,1024]{1,0:T(8,128)(2,1)S(1)}, u32[]{:S(2)}, u32[]{:S(2)}) %collective-permute-start.20) | collective-permute-done | bytes 131104 | tf_op jit(solution)/shard_map/ppermute | solution.py:39
  106.3 0.6 collective-permute-done.21.refs_3_
  107.0 0.8 join.3
  (21 shorter events, 0.1 us)
Async XLA Ops:
  0.5 1.0 copy-start
  1.5 0.9 copy-start.1
  2.4 0.9 copy-start.2
  3.3 0.9 copy-start.3
  4.2 0.7 copy-start.4
  4.9 0.7 copy-start.5
  7.3 17.3 %all-to-all-start = ((bf16[4,128,256]{2,1,0:T(8,128)(2,1)}), bf16[4,128,256]{2,1,0:T(8,128)(2,1)S(1)}, u32[]{:S(2)}, u32[]{:S(2)}) async-start(bf16[4,128,256]{2,1,0:T(8,128)(2,1)} %get-tuple-element.28), calls=%async_computation | async-start | bytes 524288 | tf_op jit(solution)/shard_map/all_to_all | solution.py:283
  12.6 9.3 %collective-permute-start.10 = (bf16[32,2048]{1,0:T(8,128)(2,1)S(1)}, bf16[32,2048]{1,0:T(8,128)(2,1)S(1)}, u32[]{:S(2)}, u32[]{:S(2)}) collective-permute-start(bf16[32,2048]{1,0:T(8,128)(2,1)S(1)} %get-tuple-element.31.refs_0_), channel_id=1, source_target_pairs={{0,24},{8,0},{16,8},{24,16},{1,25},{9,1},{17,9},{25,17},{2,26},{10... | collective-permute-start | bytes 393224 | tf_op jit(solution)/shard_map/ppermute | solution.py:39
  15.6 7.6 %collective-permute-start.11 = (bf16[32,2048]{1,0:T(8,128)(2,1)S(1)}, bf16[32,2048]{1,0:T(8,128)(2,1)S(1)}, u32[]{:S(2)}, u32[]{:S(2)}) collective-permute-start(bf16[32,2048]{1,0:T(8,128)(2,1)S(1)} %get-tuple-element.31.refs_0_), channel_id=1, source_target_pairs={{0,16},{8,24},{16,0},{24,8},{1,17},{9,25},{17,1},{25,9},{2,18},{10... | collective-permute-start | bytes 393224 | tf_op jit(solution)/shard_map/ppermute | solution.py:39
  16.2 8.4 %collective-permute-start.9 = (bf16[32,2048]{1,0:T(8,128)(2,1)S(1)}, bf16[32,2048]{1,0:T(8,128)(2,1)S(1)}, u32[]{:S(2)}, u32[]{:S(2)}) collective-permute-start(bf16[32,2048]{1,0:T(8,128)(2,1)S(1)} %get-tuple-element.31.refs_0_), channel_id=1, source_target_pairs={{0,8},{8,16},{16,24},{24,0},{1,9},{9,17},{17,25},{25,1},{2,10},{10... | collective-permute-start | bytes 393224 | tf_op jit(solution)/shard_map/ppermute | solution.py:39
  17.2 11.7 %collective-permute-start = (bf16[128,512]{1,0:T(8,128)(2,1)S(1)}, bf16[128,512]{1,0:T(8,128)(2,1)S(1)}, u32[]{:S(2)}, u32[]{:S(2)}) collective-permute-start(bf16[128,512]{1,0:T(8,128)(2,1)S(1)} %get-tuple-element.25), channel_id=1, source_target_pairs={{0,32},{32,64},{64,96},{96,0},{1,33},{33,65},{65,97},{97,1},{2,34}... | collective-permute-start | bytes 393224 | tf_op jit(solution)/shard_map/ppermute | solution.py:39
  19.2 9.6 %collective-permute-start.1 = (bf16[128,512]{1,0:T(8,128)(2,1)S(1)}, bf16[128,512]{1,0:T(8,128)(2,1)S(1)}, u32[]{:S(2)}, u32[]{:S(2)}) collective-permute-start(bf16[128,512]{1,0:T(8,128)(2,1)S(1)} %get-tuple-element.26), channel_id=1, source_target_pairs={{0,64},{32,96},{64,0},{96,32},{1,65},{33,97},{65,1},{97,33},{2,66}... | collective-permute-start | bytes 393224 | tf_op jit(solution)/shard_map/ppermute | solution.py:39
  24.6 21.7 %collective-permute-start.12 = (bf16[128,2048]{1,0:T(8,128)(2,1)S(1)}, bf16[128,2048]{1,0:T(8,128)(2,1)S(1)}, u32[]{:S(2)}, u32[]{:S(2)}) collective-permute-start(bf16[128,2048]{1,0:T(8,128)(2,1)S(1)} %stack.1.refs_0_), channel_id=1, source_target_pairs={{0,2},{2,4},{4,6},{6,0},{1,3},{3,5},{5,7},{7,1},{8,10},{10,12},{12... | collective-permute-start | bytes 1572872 | tf_op jit(solution)/shard_map/ppermute | solution.py:39
  26.2 20.6 %collective-permute-start.13 = (bf16[128,2048]{1,0:T(8,128)(2,1)S(1)}, bf16[128,2048]{1,0:T(8,128)(2,1)S(1)}, u32[]{:S(2)}, u32[]{:S(2)}) collective-permute-start(bf16[128,2048]{1,0:T(8,128)(2,1)S(1)} %stack.1.refs_0_), channel_id=1, source_target_pairs={{0,6},{2,0},{4,2},{6,4},{1,7},{3,1},{5,3},{7,5},{8,14},{10,8},{12,... | collective-permute-start | bytes 1572872 | tf_op jit(solution)/shard_map/ppermute | solution.py:39
  26.7 24.5 %collective-permute-start.14 = (bf16[128,2048]{1,0:T(8,128)(2,1)S(1)}, bf16[128,2048]{1,0:T(8,128)(2,1)S(1)}, u32[]{:S(2)}, u32[]{:S(2)}) collective-permute-start(bf16[128,2048]{1,0:T(8,128)(2,1)S(1)} %stack.1.refs_0_), channel_id=1, source_target_pairs={{0,4},{2,6},{4,0},{6,2},{1,5},{3,7},{5,1},{7,3},{8,12},{10,14},{12... | collective-permute-start | bytes 1572872 | tf_op jit(solution)/shard_map/ppermute | solution.py:39
  28.9 8.7 %collective-permute-start.3 = (bf16[4,128,256]{2,1,0:T(8,128)(2,1)S(1)}, bf16[4,128,256]{2,1,0:T(8,128)(2,1)S(1)}, u32[]{:S(2)}, u32[]{:S(2)}) collective-permute-start(bf16[4,128,256]{2,1,0:T(8,128)(2,1)S(1)} %all-to-all-done.refs_4_._), channel_id=1, source_target_pairs={{0,8},{8,16},{16,24},{24,0},{1,9},{9,17},{17,25},{25,1},{2,10},{10... | collective-permute-start | bytes 786440 | tf_op jit(solution)/shard_map/ppermute | solution.py:39
  28.9 5.5 %collective-permute-start.2 = (bf16[128,512]{1,0:T(8,128)(2,1)S(1)}, bf16[128,512]{1,0:T(8,128)(2,1)S(1)}, u32[]{:S(2)}, u32[]{:S(2)}) collective-permute-start(bf16[128,512]{1,0:T(8,128)(2,1)S(1)} %get-tuple-element.27), channel_id=1, source_target_pairs={{0,96},{32,0},{64,32},{96,64},{1,97},{33,1},{65,33},{97,65},{2,98}... | collective-permute-start | bytes 393224 | tf_op jit(solution)/shard_map/ppermute | solution.py:39
  34.4 11.9 %collective-permute-start.4 = (bf16[4,128,256]{2,1,0:T(8,128)(2,1)S(1)}, bf16[4,128,256]{2,1,0:T(8,128)(2,1)S(1)}, u32[]{:S(2)}, u32[]{:S(2)}) collective-permute-start(bf16[4,128,256]{2,1,0:T(8,128)(2,1)S(1)} %all-to-all-done.refs_4_._), channel_id=1, source_target_pairs={{0,24},{8,0},{16,8},{24,16},{1,25},{9,1},{17,9},{25,17},{2,26},{10... | collective-permute-start | bytes 786440 | tf_op jit(solution)/shard_map/ppermute | solution.py:39
  37.6 13.7 %collective-permute-start.5 = (bf16[4,128,256]{2,1,0:T(8,128)(2,1)S(1)}, bf16[4,128,256]{2,1,0:T(8,128)(2,1)S(1)}, u32[]{:S(2)}, u32[]{:S(2)}) collective-permute-start(bf16[4,128,256]{2,1,0:T(8,128)(2,1)S(1)} %all-to-all-done.refs_4_._), channel_id=1, source_target_pairs={{0,16},{8,24},{16,0},{24,8},{1,17},{9,25},{17,1},{25,9},{2,18},{10... | collective-permute-start | bytes 786440 | tf_op jit(solution)/shard_map/ppermute | solution.py:39
  46.3 12.9 %collective-permute-start.15 = (bf16[128,2048]{1,0:T(8,128)(2,1)S(1)}, bf16[128,2048]{1,0:T(8,128)(2,1)S(1)}, u32[]{:S(2)}, u32[]{:S(2)}) collective-permute-start(bf16[128,2048]{1,0:T(8,128)(2,1)S(1)} %stack.1.refs_0_), channel_id=1, source_target_pairs={{0,1},{1,0},{2,3},{3,2},{4,5},{5,4},{6,7},{7,6},{8,9},{9,8},{10,11... | collective-permute-start | bytes 1572872 | tf_op jit(solution)/shard_map/ppermute | solution.py:290
  46.3 29.3 %collective-permute-start.16 = (bf16[128,2048]{1,0:T(8,128)(2,1)S(1)}, bf16[128,2048]{1,0:T(8,128)(2,1)S(1)}, u32[]{:S(2)}, u32[]{:S(2)}) collective-permute-start(bf16[128,2048]{1,0:T(8,128)(2,1)S(1)} %collective-permute-done.12.refs_1_), channel_id=1, source_target_pairs={{0,1},{1,0},{2,3},{3,2},{4,5},{5,4},{6,7},{7,6},{8,9},{9,8},{10,11... | collective-permute-start | bytes 1572872 | tf_op jit(solution)/shard_map/ppermute | solution.py:290
  46.8 29.7 %collective-permute-start.17 = (bf16[128,2048]{1,0:T(8,128)(2,1)S(1)}, bf16[128,2048]{1,0:T(8,128)(2,1)S(1)}, u32[]{:S(2)}, u32[]{:S(2)}) collective-permute-start(bf16[128,2048]{1,0:T(8,128)(2,1)S(1)} %collective-permute-done.13.refs_2_), channel_id=1, source_target_pairs={{0,1},{1,0},{2,3},{3,2},{4,5},{5,4},{6,7},{7,6},{8,9},{9,8},{10,11... | collective-permute-start | bytes 1572872 | tf_op jit(solution)/shard_map/ppermute | solution.py:290
  51.3 27.9 %collective-permute-start.18 = (bf16[128,2048]{1,0:T(8,128)(2,1)S(1)}, bf16[128,2048]{1,0:T(8,128)(2,1)S(1)}, u32[]{:S(2)}, u32[]{:S(2)}) collective-permute-start(bf16[128,2048]{1,0:T(8,128)(2,1)S(1)} %collective-permute-done.14.refs_3_), channel_id=1, source_target_pairs={{0,1},{1,0},{2,3},{3,2},{4,5},{5,4},{6,7},{7,6},{8,9},{9,8},{10,11... | collective-permute-start | bytes 1572872 | tf_op jit(solution)/shard_map/ppermute | solution.py:290
  57.7 10.0 %collective-permute-start.22 = (bf16[256,512]{1,0:T(8,128)(2,1)S(1)}, bf16[256,512]{1,0:T(8,128)(2,1)S(1)}, u32[]{:S(2)}, u32[]{:S(2)}) collective-permute-start(bf16[256,512]{1,0:T(8,128)(2,1)S(1)} %get-tuple-element.36.x0), channel_id=1, source_target_pairs={{0,32},{32,64},{64,96},{96,0},{1,33},{33,65},{65,97},{97,1},{2,34}... | collective-permute-start | bytes 786440 | tf_op jit(solution)/shard_map/ppermute | solution.py:39
  59.2 20.8 %collective-permute-start.23 = (bf16[256,512]{1,0:T(8,128)(2,1)S(1)}, bf16[256,512]{1,0:T(8,128)(2,1)S(1)}, u32[]{:S(2)}, u32[]{:S(2)}) collective-permute-start(bf16[256,512]{1,0:T(8,128)(2,1)S(1)} %get-tuple-element.36.x0), channel_id=1, source_target_pairs={{0,96},{32,0},{64,32},{96,64},{1,97},{33,1},{65,33},{97,65},{2,98}... | collective-permute-start | bytes 786440 | tf_op jit(solution)/shard_map/ppermute | solution.py:39
  67.7 12.4 %collective-permute-start.24 = (bf16[256,512]{1,0:T(8,128)(2,1)S(1)}, bf16[256,512]{1,0:T(8,128)(2,1)S(1)}, u32[]{:S(2)}, u32[]{:S(2)}) collective-permute-start(bf16[256,512]{1,0:T(8,128)(2,1)S(1)} %get-tuple-element.36.x0), channel_id=1, source_target_pairs={{0,64},{32,96},{64,0},{96,32},{1,65},{33,97},{65,1},{97,33},{2,66}... | collective-permute-start | bytes 786440 | tf_op jit(solution)/shard_map/ppermute | solution.py:39
  75.7 15.0 %collective-permute-start.6 = (bf16[256,512]{1,0:T(8,128)(2,1)S(1)}, bf16[256,512]{1,0:T(8,128)(2,1)S(1)}, u32[]{:S(2)}, u32[]{:S(2)}) collective-permute-start(bf16[256,512]{1,0:T(8,128)(2,1)S(1)} %attend.3._.x0), channel_id=1, source_target_pairs={{0,32},{32,64},{64,96},{96,0},{1,33},{33,65},{65,97},{97,1},{2,34}... | collective-permute-start | bytes 786440 | tf_op jit(solution)/shard_map/ppermute | solution.py:39
  76.5 16.9 %collective-permute-start.7 = (bf16[256,512]{1,0:T(8,128)(2,1)S(1)}, bf16[256,512]{1,0:T(8,128)(2,1)S(1)}, u32[]{:S(2)}, u32[]{:S(2)}) collective-permute-start(bf16[256,512]{1,0:T(8,128)(2,1)S(1)} %attend.3._.x0), channel_id=1, source_target_pairs={{0,96},{32,0},{64,32},{96,64},{1,97},{33,1},{65,33},{97,65},{2,98}... | collective-permute-start | bytes 786440 | tf_op jit(solution)/shard_map/ppermute | solution.py:39
  79.2 14.2 %collective-permute-start.8 = (bf16[256,512]{1,0:T(8,128)(2,1)S(1)}, bf16[256,512]{1,0:T(8,128)(2,1)S(1)}, u32[]{:S(2)}, u32[]{:S(2)}) collective-permute-start(bf16[256,512]{1,0:T(8,128)(2,1)S(1)} %attend.3._.x0), channel_id=1, source_target_pairs={{0,64},{32,96},{64,0},{96,32},{1,65},{33,97},{65,1},{97,33},{2,66}... | collective-permute-start | bytes 786440 | tf_op jit(solution)/shard_map/ppermute | solution.py:39
  83.2 18.7 %collective-permute-start.25 = (bf16[64,1024]{1,0:T(8,128)(2,1)S(1)}, bf16[64,1024]{1,0:T(8,128)(2,1)S(1)}, u32[]{:S(2)}, u32[]{:S(2)}) collective-permute-start(bf16[64,1024]{1,0:T(8,128)(2,1)S(1)} %get-tuple-element.38), channel_id=1, source_target_pairs={{0,32},{32,64},{64,96},{96,0},{1,33},{33,65},{65,97},{97,1},{2,34}... | collective-permute-start | bytes 393224 | tf_op jit(solution)/shard_map/ppermute | solution.py:39
  83.7 18.3 %collective-permute-start.26 = (bf16[64,1024]{1,0:T(8,128)(2,1)S(1)}, bf16[64,1024]{1,0:T(8,128)(2,1)S(1)}, u32[]{:S(2)}, u32[]{:S(2)}) collective-permute-start(bf16[64,1024]{1,0:T(8,128)(2,1)S(1)} %get-tuple-element.39), channel_id=1, source_target_pairs={{0,64},{32,96},{64,0},{96,32},{1,65},{33,97},{65,1},{97,33},{2,66}... | collective-permute-start | bytes 393224 | tf_op jit(solution)/shard_map/ppermute | solution.py:39
  90.7 11.3 %collective-permute-start.27 = (bf16[64,1024]{1,0:T(8,128)(2,1)S(1)}, bf16[64,1024]{1,0:T(8,128)(2,1)S(1)}, u32[]{:S(2)}, u32[]{:S(2)}) collective-permute-start(bf16[64,1024]{1,0:T(8,128)(2,1)S(1)} %get-tuple-element.40), channel_id=1, source_target_pairs={{0,96},{32,0},{64,32},{96,64},{1,97},{33,1},{65,33},{97,65},{2,98}... | collective-permute-start | bytes 393224 | tf_op jit(solution)/shard_map/ppermute | solution.py:39
  96.6 6.8 %collective-permute-start.19 = (bf16[64,1024]{1,0:T(8,128)(2,1)S(1)}, bf16[64,1024]{1,0:T(8,128)(2,1)S(1)}, u32[]{:S(2)}, u32[]{:S(2)}) collective-permute-start(bf16[64,1024]{1,0:T(8,128)(2,1)S(1)} %get-tuple-element.33), channel_id=1, source_target_pairs={{0,32},{32,64},{64,96},{96,0},{1,33},{33,65},{65,97},{97,1},{2,34}... | collective-permute-start | bytes 393224 | tf_op jit(solution)/shard_map/ppermute | solution.py:39
  96.7 9.6 %collective-permute-start.20 = (bf16[64,1024]{1,0:T(8,128)(2,1)S(1)}, bf16[64,1024]{1,0:T(8,128)(2,1)S(1)}, u32[]{:S(2)}, u32[]{:S(2)}) collective-permute-start(bf16[64,1024]{1,0:T(8,128)(2,1)S(1)} %get-tuple-element.34), channel_id=1, source_target_pairs={{0,64},{32,96},{64,0},{96,32},{1,65},{33,97},{65,1},{97,33},{2,66}... | collective-permute-start | bytes 393224 | tf_op jit(solution)/shard_map/ppermute | solution.py:39
  102.0 5.0 %collective-permute-start.21 = (bf16[64,1024]{1,0:T(8,128)(2,1)S(1)}, bf16[64,1024]{1,0:T(8,128)(2,1)S(1)}, u32[]{:S(2)}, u32[]{:S(2)}) collective-permute-start(bf16[64,1024]{1,0:T(8,128)(2,1)S(1)} %get-tuple-element.35), channel_id=1, source_target_pairs={{0,96},{32,0},{64,32},{96,64},{1,97},{33,1},{65,33},{97,65},{2,98}... | collective-permute-start | bytes 393224 | tf_op jit(solution)/shard_map/ppermute | solution.py:39

commit v2 on v1

--- a/solution.py
+++ b/solution.py
@@ -17,6 +17,7 @@
 NORM_EPS = 1e-05
 BLOCK = 128
 SEQ = 2048
+TILE = 256
 PARTS = 2
 
 VM = pl.BlockSpec(memory_space=pltpu.VMEM)
@@ -46,13 +47,19 @@
 ORDER = (0, 3, 1, 2)
 
 
-def rotate_kernel(lambdas, gain_ref, q_ref, k_ref, v_ref, w_ref, cos_ref, sin_ref, kv_out, w_out, const_out, *q_out):
+HBM = pl.BlockSpec(memory_space=pltpu.HBM)
+
+
+def rotate_kernel(small_ref, q_hbm, k_hbm, v_hbm, cos_ref, sin_ref, kv_out, const_out, q0, q1, q2, q3, q_ref, k_ref, sems):
     z = lax.axis_index("z")
-    const_out[:1] = gain_ref[...]
-    for h in range(4):
-        const_out[h + 1 : h + 2] = jnp.full((1, 128), lambdas[z * 4 + h], F32)
-    const_out[5:] = jnp.zeros((3, 128), F32)
-    w_out[...] = w_ref[...]
+    copies = [pltpu.make_async_copy(k_hbm.at[0], k_ref, sems.at[0])]
+    for g in range(4):
+        copies.append(
+            pltpu.make_async_copy(v_hbm.at[0, :, pl.ds(g * 128, 128)], kv_out.at[g, :, pl.ds(128, 128)], sems.at[1 + g])
+        )
+    copies.append(pltpu.make_async_copy(q_hbm.at[0], q_ref, sems.at[5]))
+    for copy in copies:
+        copy.start()
     cosine = cos_ref[...]
     sine = sin_ref[...]
     lane = lax.broadcasted_iota(jnp.int32, (BLOCK, 128), 1)
@@ -63,36 +70,47 @@
         other = jnp.where(low, pltpu.roll(x, 96, 1), pltpu.roll(x, 32, 1))
         return (x * cosine + other * sine).astype(BF16)
 
+    at = lax.broadcasted_iota(jnp.int32, (8, 128), 1) - lax.broadcasted_iota(jnp.int32, (8, 128), 0)
+    own = jnp.where(at == z * 4, jnp.broadcast_to(small_ref[:1], (8, 128)), 0.0)
+    const_out[:8] = jnp.broadcast_to(jnp.sum(own, 1, keepdims=True), (8, 128))
+    const_out[8:] = jnp.broadcast_to(small_ref[1:], (8, 128))
+    copies[0].wait()
     for g in range(4):
-        kv_out[g, :, :128] = turn(k_ref[0, :, g * 128 : (g + 1) * 128])
-        kv_out[g, :, 128:] = v_ref[0, :, g * 128 : (g + 1) * 128]
-    for r in range(4):
+        kv_out[g, :, :128] = turn(k_ref[:, g * 128 : (g + 1) * 128])
+    copies[5].wait()
+    for r, q_out in enumerate((q0, q1, q2, q3)):
         group = lax.rem(z + r, 4) * 512
         for h in range(4):
             at = pl.multiple_of(group + h * 128, 128)
-            q_out[r][:, h * 128 : (h + 1) * 128] = turn(q_ref[0, :, pl.ds(at, 128)]) * BF16(0.125)
-
-
-def rotate(lambdas, gain, q, k, v, w, cosine, sine):
+            q_out[:, h * 128 : (h + 1) * 128] = turn(q_ref[:, pl.ds(at, 128)]) * BF16(0.125)
+    for copy in copies[1:5]:
+        copy.wait()
+
+
+def rotate(small, q, k, v, cosine, sine):
     return pl.pallas_call(
         rotate_kernel,
-        in_specs=[SM] + [VM] * 7,
-        out_specs=[VM] * 7,
-        out_shape=[shape(4, BLOCK, 256), shape(*w.shape), jax.ShapeDtypeStruct((8, 128), F32)]
-        + [shape(BLOCK, 512)] * 4,
+        in_specs=[VM] + [HBM] * 3 + [VM] * 2,
+        out_specs=[VM] * 6,
+        out_shape=[shape(4, BLOCK, 256), jax.ShapeDtypeStruct((16, 128), F32)] + [shape(BLOCK, 512)] * 4,
+        scratch_shapes=[
+            pltpu.VMEM((BLOCK, 2048), BF16),
+            pltpu.VMEM((BLOCK, 512), BF16),
+            pltpu.SemaphoreType.DMA((6,)),
+        ],
         cost_estimate=cost(2**20, 2**20),
-        compiler_params=room(8),
+        compiler_params=pltpu.CompilerParams(vmem_limit_bytes=54500 * 1024),
         name="rotate",
-    )(lambdas, gain, q, k, v, w, cosine, sine)
+    )(small, q, k, v, cosine, sine)
 
 
 def attend_kernel(rows, const, *refs):
     z = lax.axis_index("z")
     y = lax.axis_index("y")
-    gain = const[:1]
     q_refs, refs = refs[:4], refs[4:]
-    if len(refs) == 8:
-        kv_refs, (out_ref, kbuf, vbuf, q_ref) = refs[:4], refs[4:]
+    q_ref, sbuf, ebuf, bias = refs[-4:]
+    if len(refs) == 11:
+        kv_refs, (out_ref, kbuf, vbuf) = refs[:4], refs[4:7]
         for r, ref in enumerate(kv_refs):
             src = lax.rem(y + ORDER[r], 4)
             for j in range(4):
@@ -100,51 +118,86 @@
                 kbuf[:, pl.ds(at, 128)] = ref[j, :, :128].T
                 vbuf[pl.ds(at, 128), :] = ref[j, :, 128:]
     else:
-        kbuf, vbuf, out_ref, q_ref = refs
+        kbuf, vbuf, out_ref = refs[:3]
     for r, ref in enumerate(q_refs):
         q_ref[lax.rem(z + 4 - r, 4)] = ref[rows, :]
+
     count = rows.stop - rows.start
     heads = BLOCK // count
     first = lax.broadcasted_iota(jnp.int32, (count, 128), 1) < HEAD_DIM
     zero = jnp.zeros((count, 128), BF16)
     key_at = lax.broadcasted_iota(jnp.int32, (2 * BLOCK, 512), 1)
     query_at = lax.broadcasted_iota(jnp.int32, (2 * BLOCK, 512), 0) % count + rows.start
-    allowed = key_at <= query_at + y * BLOCK
+    bias[...] = jnp.where(key_at <= query_at + y * BLOCK, 0.0, -jnp.inf)
     row_head = lax.broadcasted_iota(jnp.int32, (BLOCK, 1), 0) // count
-
-    for i in range(4):
+    steps = [(i, g) for i in range(4) for g in range(4 // heads)]
+
+    def query(n):
+        i, g = steps[n]
+        qs = [q_ref[i, :, h * 128 : (h + 1) * 128] for h in range(g * heads, (g + 1) * heads)]
+        return jnp.concatenate([jnp.where(first, q, zero) for q in qs] + [jnp.where(first, zero, q) for q in qs], 0)
+
+    def score(n, q, t):
+        i = steps[n][0]
+        s = jnp.dot(q, kbuf[:, t * TILE : (t + 1) * TILE], preferred_element_type=F32)
+        edge = t * TILE - i * 512
+        if edge >= 0:
+            s = s + bias[:, edge : edge + TILE]
+        sbuf[n % 3, :, t * TILE : (t + 1) * TILE] = s
+
+    def tops(n):
+        reach = (steps[n][0] + 1) * 512
+        return jnp.max(sbuf[n % 3, :, :reach], 1, keepdims=True)
+
+    def totals(n):
+        reach = (steps[n][0] + 1) * 512
+        return 1.0 / jnp.sum(sbuf[n % 3, :, :reach], 1, keepdims=True)
+
+    def blend(n, scale, t):
+        at = slice(t * TILE, (t + 1) * TILE)
+        w = sbuf[n % 3, :BLOCK, at] * scale[0] - sbuf[n % 3, BLOCK:, at] * scale[1]
+        ebuf[n % 2, :, at] = w.astype(BF16)
+
+    def factor(n):
+        g = steps[n][1]
+        factor = const[g * heads : g * heads + 1, :1]
+        if heads == 2:
+            factor = jnp.where(row_head == 0, factor, const[g * heads + 1 : g * heads + 2, :1])
+        return factor
+
+    def finish(n):
+        i, g = steps[n]
         reach = (i + 1) * 512
-        for g in range(4 // heads):
-            qs = [q_ref[i, :, h * 128 : (h + 1) * 128] for h in range(g * heads, (g + 1) * heads)]
-            q = jnp.concatenate([jnp.where(first, q, zero) for q in qs] + [jnp.where(first, zero, q) for q in qs], 0)
-            last = jnp.dot(q, kbuf[:, reach - 512 : reach], preferred_element_type=F32)
-            last = jnp.where(allowed, last, -jnp.inf)
-            top = jnp.max(last, 1, keepdims=True)
-            if i:
-                rest = jnp.dot(q, kbuf[:, : reach - 512], preferred_element_type=F32)
-                top = jnp.maximum(top, jnp.max(rest, 1, keepdims=True))
-                rest = jnp.exp(rest - top)
-            last = jnp.exp(last - top)
-            total = jnp.sum(last, 1, keepdims=True)
-            if i:
-                total = total + jnp.sum(rest, 1, keepdims=True)
-            scale = 1.0 / total
-            one = scale[:BLOCK]
-            factor = const[g * heads + 1 : g * heads + 2, :1]
-            if heads == 2:
-                factor = jnp.where(row_head == 0, factor, const[g * heads + 2 : g * heads + 3, :1])
-            two = scale[BLOCK:] * factor
-            w = (last[:BLOCK] * one - last[BLOCK:] * two).astype(BF16)
-            acc = jnp.dot(w, vbuf[reach - 512 : reach], preferred_element_type=F32)
-            if i:
-                w = (rest[:BLOCK] * one - rest[BLOCK:] * two).astype(BF16)
-                acc = acc + jnp.dot(w, vbuf[: reach - 512], preferred_element_type=F32)
-            square = jnp.mean(acc * acc, 1, keepdims=True)
-            acc = acc * (lax.rsqrt(square + NORM_EPS) * OUTPUT_SCALE) * gain
-            acc = acc.astype(BF16)
-            for k in range(heads):
-                h = g * heads + k
-                out_ref[i * count : (i + 1) * count, h * 128 : (h + 1) * 128] = acc[k * count : (k + 1) * count]
+        acc = jnp.dot(ebuf[n % 2, :, :reach], vbuf[:reach], preferred_element_type=F32)
+        square = jnp.mean(acc * acc, 1, keepdims=True)
+        acc = acc * (lax.rsqrt(square + NORM_EPS) * OUTPUT_SCALE) * const[8:9]
+        acc = acc.astype(BF16)
+        for k in range(heads):
+            h = g * heads + k
+            out_ref[i * count : (i + 1) * count, h * 128 : (h + 1) * 128] = acc[k * count : (k + 1) * count]
+
+    last = len(steps) - 1
+    tiles = [(i + 1) * 512 // TILE for i, _ in steps]
+    top, scale = {}, {}
+    for n in range(-1, last + 2):
+        if n < last:
+            q = query(n + 1)
+        span = max(tiles[k] for k in (n - 1, n, n + 1) if 0 <= k <= last)
+        for t in range(span):
+            if n < last and t < tiles[n + 1]:
+                score(n + 1, q, t)
+            if 0 <= n <= last and t < tiles[n]:
+                at = slice(t * TILE, (t + 1) * TILE)
+                sbuf[n % 3, :, at] = jnp.exp(sbuf[n % 3, :, at] - top[n])
+            if n >= 1 and t < tiles[n - 1]:
+                blend(n - 1, scale[n - 1], t)
+        if n < last:
+            top[n + 1] = tops(n + 1)
+        if 0 <= n <= last:
+            total = totals(n)
+            scale[n] = total[:BLOCK], total[BLOCK:] * factor(n)
+        if n >= 1:
+            finish(n - 1)
 
 
 def attend(rows, const, q, keys):
@@ -157,8 +210,13 @@
         in_specs=[VM] * (5 + len(keys)),
         out_specs=[VM] * len(outs),
         out_shape=outs,
-        scratch_shapes=[pltpu.VMEM((4, count, 512), BF16)],
-        compiler_params=room(16),
+        scratch_shapes=[
+            pltpu.VMEM((4, count, 512), BF16),
+            pltpu.VMEM((3, 2 * BLOCK, SEQ), F32),
+            pltpu.VMEM((2, BLOCK, SEQ), BF16),
+            pltpu.VMEM((2 * BLOCK, 512), F32),
+        ],
+        compiler_params=room(20),
         cost_estimate=cost(2**31, 2**22),
         name="attend",
     )(const, *q, *keys)
@@ -219,18 +277,16 @@
     count = x0.shape[0] // 4
     for r, ref in enumerate((x0, x1, x2, x3)):
         at = pl.multiple_of(lax.rem(z + ORDER[r], 4) * 512, 512)
-        xbuf[:, pl.ds(at, 512)] = ref[...]
+        for d in range(4):
+            row = pl.multiple_of(lax.rem(z + d, 4) * count, count)
+            xbuf[d * count : (d + 1) * count, pl.ds(at, 512)] = ref[pl.ds(row, count), :]
     for n in range(4):
         cols = slice(n * 256, (n + 1) * 256)
         part = lax.dot_general(
             xbuf[...], wbuf[cols, :], (((1,), (1,)), ((), ())), preferred_element_type=F32
         ).astype(BF16)
-        for i in range(4):
-            for r in range(4):
-
-                @pl.when(lax.rem(i + 4 - z, 4) == r)
-                def _():
-                    outs[r][:, cols] = part[i * count : (i + 1) * count]
+        for d in range(4):
+            outs[d][:, cols] = part[d * count : (d + 1) * count]
 
 
 def project(after, xs, weights):
@@ -277,14 +333,14 @@
     cosine = jnp.cos(angles)
     sign = jnp.where(jnp.arange(128) % HEAD_DIM < HEAD_DIM // 2, -1.0, 1.0).astype(F32)
     sine = jnp.sin(angles) * sign[None, :]
-    gain = value_gain.reshape(1, 128)
-    kv_split, wt, const, *q_split = rotate(lambdas, gain, queries, keys, values, out_weight.T, cosine, sine)
+    small = jnp.stack([jnp.pad(lambdas, (0, 128 - lambdas.shape[0])), value_gain])
+    wy = line("y", out_weight.T)
+    kv_split, const, *q_split = rotate(small, queries, keys, values, cosine, sine)
 
     kv_line = lax.all_to_all(kv_split, "z", 0, 0)
     kv_all = line("y", kv_line)
     q = [q_split[0]] + [hop("z", r, q_split[r]) for r in (1, 2, 3)]
 
-    wy = line("y", wt)
     wy = stack(kv_line, wy)
     wx = line("x", wy)
     wc = tuple(lax.ppermute(p, "c", [(0, 1), (1, 0)]) for p in wx)

time: 109 us -> 101 us (0.927)
  Pallas kernels: 22.7 us -> 16.2 us
  local copies, waits for them, and re-layouts: 5.14 us -> 1.65 us
  waiting for transfers between devices: 36.2 us -> 38.2 us
    unnamed x12 -> x2, local copies, waits for them, and re-layouts: 5.06 us -> 0.91 us
    pallas_call x2, Pallas kernels: 6.3 us -> 2.62 us  [project(): pl.pallas_call(project_kernel, in_specs=[ANY] + [VM] * 5, out_specs=[VM]...]
    pallas_call x2, Pallas kernels: 12.6 us -> 9.17 us  [attend(): pl.pallas_call(functools.partial(attend_kernel, rows), in_specs=[VM] * (5...]
    ppermute x24, waiting for transfers between devices: 36.2 us -> 38.2 us  [hop(): return lax.ppermute(x, axis, [(i, (i + step) % 4) for i in range(4)])]
  transfers between devices with their start and end apart: 29 -> 29, of which waited for: 11 -> 11; matrix products, arithmetic and copies ran while one was open for 0% -> 0% of each run, Pallas kernels for 19% -> 13%
where the time goes in v2:
time: 101 us; the launch traced here: 100 us
  starting transfers between devices  43.1 us (43%)
  waiting for transfers between devices  38.2 us (38%)
  Pallas kernels  16.2 us (16%)
  local copies, waits for them, and re-layouts  1.65 us (2%)
    ppermute x24, waiting for transfers between devices, hop(): return lax.ppermute(x, axis, [(i, (i + step) % 4) for i in range(4)])  38.2 us
    ppermute x24, starting transfers between devices, hop(): return lax.ppermute(x, axis, [(i, (i + step) % 4) for i in range(4)])  37.2 us
    pallas_call x2, Pallas kernels, attend(): pl.pallas_call(functools.partial(attend_kernel, rows), in_specs=[VM] * (5...  9.17 us
    all_to_all x1, starting transfers between devices, shards(): kv_line = lax.all_to_all(kv_split, 'z', 0, 0)  5.32 us
    pallas_call x2, Pallas kernels, project(): pl.pallas_call(project_kernel, in_specs=[ANY] + [VM] * 5, out_specs=[VM]...  2.62 us
    pallas_call x1, Pallas kernels, rotate(): pl.pallas_call(rotate_kernel, in_specs=[VM] + [HBM] * 3 + [VM] * 2, out_s...  2.38 us
  transfers between devices with their start and end apart: 29, of which 11 were waited for; matrix products, arithmetic and copies ran while one was open for 0% of the time, Pallas kernels for 13%

profile of v2, /device:TPU:2, one launch (start us, length us, event | category | flops | bytes accessed | tf_op | source)
XLA Modules:
  0.0 100.2 jit_solution(8049656805011099864)
XLA Ops:
  0.1 0.1 mul.44
  0.1 0.7 pad_bitcast_fusion
  0.8 0.7 pad_maximum_fusion.small_ref
  1.5 0.3 fusion
  1.8 2.4 %rotate.1 = (bf16[4,128,256]{2,1,0:T(8,128)(2,1)}, f32[16,128]{1,0:T(8,128)S(1)}, bf16[128,512]{1,0:T(8,128)(2,1)S(1)}, bf16[128,512]{1,0:T(8,128)(2,1)S(1)}, bf...) custom-call(f32[2,128]{1,0:T(2,128)S(1)} %pad_maximum_fusion.small_ref, bf16[1,128,2048]{2,1,0:T(8,128)(2,1)} %q_hbm.1, ...), custom_call_target="tpu_custom_call" | custom-call | flops 1048576 | bytes 1048576 | tf_op jit(solution)/shard_map/rotate/pallas_call | solution.py:91
  4.2 5.3 %all-to-all-start = ((bf16[4,128,256]{2,1,0:T(8,128)(2,1)}), bf16[4,128,256]{2,1,0:T(8,128)(2,1)S(1)}, u32[]{:S(2)}, u32[]{:S(2)}) async-start(bf16[4,128,256]{2,1,0:T(8,128)(2,1)} %get-tuple-element.27), calls=%async_computation | async-start | bytes 524288 | tf_op jit(solution)/shard_map/all_to_all | solution.py:340
  9.5 3.0 %collective-permute-start.10 = (bf16[32,2048]{1,0:T(8,128)(2,1)}, bf16[32,2048]{1,0:T(8,128)(2,1)S(1)}, u32[]{:S(2)}, u32[]{:S(2)}) collective-permute-start(bf16[32,2048]{1,0:T(8,128)(2,1)} %bitcast.4), channel_id=1, source_target_pairs={{0,24},{8,0},{16,8},{24,16},{1,25},{9,1},{17,9},{25,17},{2,26},{10... | collective-permute-start | bytes 393224 | tf_op jit(solution)/shard_map/ppermute | solution.py:40
  12.5 0.6 collective-permute-start.11
  13.1 1.0 collective-permute-start.9
  14.1 2.0 %collective-permute-start = (bf16[128,512]{1,0:T(8,128)(2,1)S(1)}, bf16[128,512]{1,0:T(8,128)(2,1)S(1)}, u32[]{:S(2)}, u32[]{:S(2)}) collective-permute-start(bf16[128,512]{1,0:T(8,128)(2,1)S(1)} %get-tuple-element.24), channel_id=1, source_target_pairs={{0,32},{32,64},{64,96},{96,0},{1,33},{33,65},{65,97},{97,1},{2,34}... | collective-permute-start | bytes 393224 | tf_op jit(solution)/shard_map/ppermute | solution.py:40
  16.1 2.7 %collective-permute-start.1 = (bf16[128,512]{1,0:T(8,128)(2,1)S(1)}, bf16[128,512]{1,0:T(8,128)(2,1)S(1)}, u32[]{:S(2)}, u32[]{:S(2)}) collective-permute-start(bf16[128,512]{1,0:T(8,128)(2,1)S(1)} %get-tuple-element.25), channel_id=1, source_target_pairs={{0,64},{32,96},{64,0},{96,32},{1,65},{33,97},{65,1},{97,33},{2,66}... | collective-permute-start | bytes 393224 | tf_op jit(solution)/shard_map/ppermute | solution.py:40
  18.8 0.0 collective-permute-done.10.refs_2_
  18.8 1.5 %collective-permute-done.11.refs_3_ = bf16[32,2048]{1,0:T(8,128)(2,1)S(1)} collective-permute-done((bf16[32,2048]{1,0:T(8,128)(2,1)}, bf16[32,2048]{1,0:T(8,128)(2,1)S(1)}, u32[]{:S(2)}, u32[]{:S(2)}) %collective-permute-start.11) | collective-permute-done | bytes 131104 | tf_op jit(solution)/shard_map/ppermute | solution.py:40
  20.3 1.4 %collective-permute-done.9.refs_1_ = bf16[32,2048]{1,0:T(8,128)(2,1)S(1)} collective-permute-done((bf16[32,2048]{1,0:T(8,128)(2,1)}, bf16[32,2048]{1,0:T(8,128)(2,1)S(1)}, u32[]{:S(2)}, u32[]{:S(2)}) %collective-permute-start.9) | collective-permute-done | bytes 131104 | tf_op jit(solution)/shard_map/ppermute | solution.py:40
  21.7 0.0 all-to-all-done.refs_4_._
  21.7 0.9 copy-done
  22.6 1.6 %collective-permute-start.12 = (bf16[128,2048]{1,0:T(8,128)(2,1)S(1)}, bf16[128,2048]{1,0:T(8,128)(2,1)S(1)}, u32[]{:S(2)}, u32[]{:S(2)}) collective-permute-start(bf16[128,2048]{1,0:T(8,128)(2,1)S(1)} %stack.13.refs_0_), channel_id=1, source_target_pairs={{0,2},{2,4},{4,6},{6,0},{1,3},{3,5},{5,7},{7,1},{8,10},{10,12},{12... | collective-permute-start | bytes 1572872 | tf_op jit(solution)/shard_map/ppermute | solution.py:40
  24.2 0.5 collective-permute-start.13
  24.7 2.1 %collective-permute-start.14 = (bf16[128,2048]{1,0:T(8,128)(2,1)S(1)}, bf16[128,2048]{1,0:T(8,128)(2,1)S(1)}, u32[]{:S(2)}, u32[]{:S(2)}) collective-permute-start(bf16[128,2048]{1,0:T(8,128)(2,1)S(1)} %stack.13.refs_0_), channel_id=1, source_target_pairs={{0,4},{2,6},{4,0},{6,2},{1,5},{3,7},{5,1},{7,3},{8,12},{10,14},{12... | collective-permute-start | bytes 1572872 | tf_op jit(solution)/shard_map/ppermute | solution.py:40
  26.9 0.0 collective-permute-done.refs_1_
  26.9 0.0 collective-permute-start.3
  26.9 0.0 collective-permute-done.1.refs_2_
  26.9 3.0 %collective-permute-start.2 = (bf16[128,512]{1,0:T(8,128)(2,1)S(1)}, bf16[128,512]{1,0:T(8,128)(2,1)S(1)}, u32[]{:S(2)}, u32[]{:S(2)}) collective-permute-start(bf16[128,512]{1,0:T(8,128)(2,1)S(1)} %get-tuple-element.26), channel_id=1, source_target_pairs={{0,96},{32,0},{64,32},{96,64},{1,97},{33,1},{65,33},{97,65},{2,98}... | collective-permute-start | bytes 393224 | tf_op jit(solution)/shard_map/ppermute | solution.py:40
  29.9 2.5 %collective-permute-done.2.refs_3_ = bf16[128,512]{1,0:T(8,128)(2,1)S(1)} collective-permute-done((bf16[128,512]{1,0:T(8,128)(2,1)S(1)}, bf16[128,512]{1,0:T(8,128)(2,1)S(1)}, u32[]{:S(2)}, u32[]{:S(2)}) %collective-permute-start.2) | collective-permute-done | bytes 131104 | tf_op jit(solution)/shard_map/ppermute | solution.py:40
  32.4 3.2 %collective-permute-start.4 = (bf16[4,128,256]{2,1,0:T(8,128)(2,1)S(1)}, bf16[4,128,256]{2,1,0:T(8,128)(2,1)S(1)}, u32[]{:S(2)}, u32[]{:S(2)}) collective-permute-start(bf16[4,128,256]{2,1,0:T(8,128)(2,1)S(1)} %all-to-all-done.refs_4_._), channel_id=1, source_target_pairs={{0,24},{8,0},{16,8},{24,16},{1,25},{9,1},{17,9},{25,17},{2,26},{10... | collective-permute-start | bytes 786440 | tf_op jit(solution)/shard_map/ppermute | solution.py:40
  35.6 0.0 collective-permute-done.3.refs_5_
  35.6 0.0 collective-permute-start.5
  35.6 8.7 %collective-permute-done.4.refs_6_ = bf16[4,128,256]{2,1,0:T(8,128)(2,1)S(1)} collective-permute-done((bf16[4,128,256]{2,1,0:T(8,128)(2,1)S(1)}, bf16[4,128,256]{2,1,0:T(8,128)(2,1)S(1)}, u32[]{:S(2)}, u32[]{:S(2)}) %collective-permute-start.4) | collective-permute-done | bytes 262176 | tf_op jit(solution)/shard_map/ppermute | solution.py:40
  44.3 0.0 collective-permute-start.15
  44.3 0.0 collective-permute-done.12.refs_1_
  44.3 0.5 collective-permute-start.16
  44.9 0.0 collective-permute-done.13.refs_2_
  44.9 0.1 collective-permute-start.17
  44.9 4.3 %collective-permute-done.14.refs_3_ = bf16[128,2048]{1,0:T(8,128)(2,1)S(1)} collective-permute-done((bf16[128,2048]{1,0:T(8,128)(2,1)S(1)}, bf16[128,2048]{1,0:T(8,128)(2,1)S(1)}, u32[]{:S(2)}, u32[]{:S(2)}) %collective-permute-start.14) | collective-permute-done | bytes 524320 | tf_op jit(solution)/shard_map/ppermute | solution.py:40
  49.3 0.0 collective-permute-start.18
  49.3 4.7 %attend.2 = (bf16[256,512]{1,0:T(8,128)(2,1)S(1)}, bf16[128,2048]{1,0:T(8,128)(2,1)S(1)}, bf16[2048,128]{1,0:T(8,128)(2,1)S(1)}) custom-call(f32[16,128]{1,0:T(8,128)S(1)} %get-tuple-element.22.const, bf16[128,512]{1,0:T(8,128)(2,1)S(1)} %get-tuple-element.23.refs_0_, bf16[128,512]{1,0:T(8,128)(2,1)S(1)} %collective-permute-done.refs_1_, ...), custom_call_target="tpu_custom_call" | custom-call | flops 2147483648 | bytes 4194304 | tf_op jit(solution)/shard_map/attend/pallas_call | solution.py:208
  54.0 1.5 %collective-permute-start.22 = (bf16[256,512]{1,0:T(8,128)(2,1)S(1)}, bf16[256,512]{1,0:T(8,128)(2,1)S(1)}, u32[]{:S(2)}, u32[]{:S(2)}) collective-permute-start(bf16[256,512]{1,0:T(8,128)(2,1)S(1)} %get-tuple-element.34.x0), channel_id=1, source_target_pairs={{0,32},{32,64},{64,96},{96,0},{1,33},{33,65},{65,97},{97,1},{2,34}... | collective-permute-start | bytes 786440 | tf_op jit(solution)/shard_map/ppermute | solution.py:40
  55.5 1.8 %collective-permute-start.23 = (bf16[256,512]{1,0:T(8,128)(2,1)S(1)}, bf16[256,512]{1,0:T(8,128)(2,1)S(1)}, u32[]{:S(2)}, u32[]{:S(2)}) collective-permute-start(bf16[256,512]{1,0:T(8,128)(2,1)S(1)} %get-tuple-element.34.x0), channel_id=1, source_target_pairs={{0,96},{32,0},{64,32},{96,64},{1,97},{33,1},{65,33},{97,65},{2,98}... | collective-permute-start | bytes 786440 | tf_op jit(solution)/shard_map/ppermute | solution.py:40
  57.3 6.7 %collective-permute-done.22.x1 = bf16[256,512]{1,0:T(8,128)(2,1)S(1)} collective-permute-done((bf16[256,512]{1,0:T(8,128)(2,1)S(1)}, bf16[256,512]{1,0:T(8,128)(2,1)S(1)}, u32[]{:S(2)}, u32[]{:S(2)}) %collective-permute-start.22) | collective-permute-done | bytes 262176 | tf_op jit(solution)/shard_map/ppermute | solution.py:40
  64.0 1.8 %collective-permute-start.24 = (bf16[256,512]{1,0:T(8,128)(2,1)S(1)}, bf16[256,512]{1,0:T(8,128)(2,1)S(1)}, u32[]{:S(2)}, u32[]{:S(2)}) collective-permute-start(bf16[256,512]{1,0:T(8,128)(2,1)S(1)} %get-tuple-element.34.x0), channel_id=1, source_target_pairs={{0,64},{32,96},{64,0},{96,32},{1,65},{33,97},{65,1},{97,33},{2,66}... | collective-permute-start | bytes 786440 | tf_op jit(solution)/shard_map/ppermute | solution.py:40
  65.7 4.5 %attend.3._.x0 = bf16[256,512]{1,0:T(8,128)(2,1)S(1)} custom-call(f32[16,128]{1,0:T(8,128)S(1)} %get-tuple-element.22.const, bf16[128,512]{1,0:T(8,128)(2,1)S(1)} %get-tuple-element.23.refs_0_, bf16[128,512]{1,0:T(8,128)(2,1)S(1)} %collective-permute-done.refs_1_, bf16[128,512]{1,0:T(8,128)(2,1)S(1)} %collective-permute-done.1.refs_2_, ...), custom_call_target="tpu_custom_call" | custom-call | flops 2147483648 | bytes 4194304 | tf_op jit(solution)/shard_map/attend/pallas_call | solution.py:208
  70.2 0.6 collective-permute-start.6
  70.9 0.0 collective-permute-done.17.refs_6_
  70.9 2.7 %collective-permute-start.7 = (bf16[256,512]{1,0:T(8,128)(2,1)S(1)}, bf16[256,512]{1,0:T(8,128)(2,1)S(1)}, u32[]{:S(2)}, u32[]{:S(2)}) collective-permute-start(bf16[256,512]{1,0:T(8,128)(2,1)S(1)} %attend.3._.x0), channel_id=1, source_target_pairs={{0,96},{32,0},{64,32},{96,64},{1,97},{33,1},{65,33},{97,65},{2,98}... | collective-permute-start | bytes 786440 | tf_op jit(solution)/shard_map/ppermute | solution.py:40
  73.5 0.0 collective-permute-done.18.refs_7_
  73.6 0.6 collective-permute-start.8
  74.1 0.3 columns.1.wbuf
  74.4 0.0 collective-permute-done.24.x3
  74.4 1.3 %project.3 = (bf16[64,1024]{1,0:T(8,128)(2,1)S(1)}, bf16[64,1024]{1,0:T(8,128)(2,1)S(1)}, bf16[64,1024]{1,0:T(8,128)(2,1)S(1)}, bf16[64,1024]{1,0:T(8,128)(2,1)S(1)}) custom-call(bf16[256,512]{1,0:T(8,128)(2,1)S(1)} %attend.3._.x0, bf16[256,512]{1,0:T(8,128)(2,1)S(1)} %get-tuple-element.34.x0, bf16[256,512]{1,0:T(8,128)(2,1)S(1)} %collective-permute-done.22.x1, ...), custom_call_target="tpu_custom_call" | custom-call | flops 1073741824 | bytes 4194304 | tf_op jit(solution)/shard_map/project/pallas_call | solution.py:294
  75.7 0.5 collective-permute-start.25
  76.2 2.7 %collective-permute-start.26 = (bf16[64,1024]{1,0:T(8,128)(2,1)S(1)}, bf16[64,1024]{1,0:T(8,128)(2,1)S(1)}, u32[]{:S(2)}, u32[]{:S(2)}) collective-permute-start(bf16[64,1024]{1,0:T(8,128)(2,1)S(1)} %get-tuple-element.37), channel_id=1, source_target_pairs={{0,64},{32,96},{64,0},{96,32},{1,65},{33,97},{65,1},{97,33},{2,66}... | collective-permute-start | bytes 393224 | tf_op jit(solution)/shard_map/ppermute | solution.py:40
  78.9 7.3 %collective-permute-done.6.x1 = bf16[256,512]{1,0:T(8,128)(2,1)S(1)} collective-permute-done((bf16[256,512]{1,0:T(8,128)(2,1)S(1)}, bf16[256,512]{1,0:T(8,128)(2,1)S(1)}, u32[]{:S(2)}, u32[]{:S(2)}) %collective-permute-start.6) | collective-permute-done | bytes 262176 | tf_op jit(solution)/shard_map/ppermute | solution.py:40
  86.1 1.6 %collective-permute-done.7.x2 = bf16[256,512]{1,0:T(8,128)(2,1)S(1)} collective-permute-done((bf16[256,512]{1,0:T(8,128)(2,1)S(1)}, bf16[256,512]{1,0:T(8,128)(2,1)S(1)}, u32[]{:S(2)}, u32[]{:S(2)}) %collective-permute-start.7) | collective-permute-done | bytes 262176 | tf_op jit(solution)/shard_map/ppermute | solution.py:40
  87.7 0.0 collective-permute-done.8.x3
  87.7 1.3 %project.2 = (bf16[64,1024]{1,0:T(8,128)(2,1)S(1)}, bf16[64,1024]{1,0:T(8,128)(2,1)S(1)}, bf16[64,1024]{1,0:T(8,128)(2,1)S(1)}, bf16[64,1024]{1,0:T(8,128)(2,1)S(1)}) custom-call(bf16[256,512]{1,0:T(8,128)(2,1)S(1)} %attend.3._.x0, bf16[256,512]{1,0:T(8,128)(2,1)S(1)} %attend.3._.x0, bf16[256,512]{1,0:T(8,128)(2,1)S(1)} %collective-permute-done.6.x1, ...), custom_call_target="tpu_custom_call" | custom-call | flops 1073741824 | bytes 4194304 | tf_op jit(solution)/shard_map/project/pallas_call | solution.py:294
  89.1 0.5 collective-permute-start.19
  89.6 4.9 %collective-permute-start.20 = (bf16[64,1024]{1,0:T(8,128)(2,1)S(1)}, bf16[64,1024]{1,0:T(8,128)(2,1)S(1)}, u32[]{:S(2)}, u32[]{:S(2)}) collective-permute-start(bf16[64,1024]{1,0:T(8,128)(2,1)S(1)} %get-tuple-element.32), channel_id=1, source_target_pairs={{0,64},{32,96},{64,0},{96,32},{1,65},{33,97},{65,1},{97,33},{2,66}... | collective-permute-start | bytes 393224 | tf_op jit(solution)/shard_map/ppermute | solution.py:40
  94.4 0.0 collective-permute-done.25.refs_1_
  94.4 0.0 collective-permute-done.27.refs_3_
  94.5 0.8 join.2.refs_4_
  95.3 0.6 collective-permute-done.19.refs_1_
  95.9 2.9 %collective-permute-done.20.refs_2_ = bf16[64,1024]{1,0:T(8,128)(2,1)S(1)} collective-permute-done((bf16[64,1024]{1,0:T(8,128)(2,1)S(1)}, bf16[64,1024]{1,0:T(8,128)(2,1)S(1)}, u32[]{:S(2)}, u32[]{:S(2)}) %collective-permute-start.20) | collective-permute-done | bytes 131104 | tf_op jit(solution)/shard_map/ppermute | solution.py:40
  98.8 0.6 collective-permute-done.21.refs_3_
  99.4 0.8 join.3
  (13 shorter events, 0.1 us)
Async XLA Ops:
  4.2 17.5 %all-to-all-start = ((bf16[4,128,256]{2,1,0:T(8,128)(2,1)}), bf16[4,128,256]{2,1,0:T(8,128)(2,1)S(1)}, u32[]{:S(2)}, u32[]{:S(2)}) async-start(bf16[4,128,256]{2,1,0:T(8,128)(2,1)} %get-tuple-element.27), calls=%async_computation | async-start | bytes 524288 | tf_op jit(solution)/shard_map/all_to_all | solution.py:340
  9.5 9.3 %collective-permute-start.10 = (bf16[32,2048]{1,0:T(8,128)(2,1)}, bf16[32,2048]{1,0:T(8,128)(2,1)S(1)}, u32[]{:S(2)}, u32[]{:S(2)}) collective-permute-start(bf16[32,2048]{1,0:T(8,128)(2,1)} %bitcast.4), channel_id=1, source_target_pairs={{0,24},{8,0},{16,8},{24,16},{1,25},{9,1},{17,9},{25,17},{2,26},{10... | collective-permute-start | bytes 393224 | tf_op jit(solution)/shard_map/ppermute | solution.py:40
  12.5 7.8 %collective-permute-start.11 = (bf16[32,2048]{1,0:T(8,128)(2,1)}, bf16[32,2048]{1,0:T(8,128)(2,1)S(1)}, u32[]{:S(2)}, u32[]{:S(2)}) collective-permute-start(bf16[32,2048]{1,0:T(8,128)(2,1)} %bitcast.5), channel_id=1, source_target_pairs={{0,16},{8,24},{16,0},{24,8},{1,17},{9,25},{17,1},{25,9},{2,18},{10... | collective-permute-start | bytes 393224 | tf_op jit(solution)/shard_map/ppermute | solution.py:40
  13.1 8.6 %collective-permute-start.9 = (bf16[32,2048]{1,0:T(8,128)(2,1)}, bf16[32,2048]{1,0:T(8,128)(2,1)S(1)}, u32[]{:S(2)}, u32[]{:S(2)}) collective-permute-start(bf16[32,2048]{1,0:T(8,128)(2,1)} %bitcast.6), channel_id=1, source_target_pairs={{0,8},{8,16},{16,24},{24,0},{1,9},{9,17},{17,25},{25,1},{2,10},{10... | collective-permute-start | bytes 393224 | tf_op jit(solution)/shard_map/ppermute | solution.py:40
  14.1 12.8 %collective-permute-start = (bf16[128,512]{1,0:T(8,128)(2,1)S(1)}, bf16[128,512]{1,0:T(8,128)(2,1)S(1)}, u32[]{:S(2)}, u32[]{:S(2)}) collective-permute-start(bf16[128,512]{1,0:T(8,128)(2,1)S(1)} %get-tuple-element.24), channel_id=1, source_target_pairs={{0,32},{32,64},{64,96},{96,0},{1,33},{33,65},{65,97},{97,1},{2,34}... | collective-permute-start | bytes 393224 | tf_op jit(solution)/shard_map/ppermute | solution.py:40
  16.1 10.8 %collective-permute-start.1 = (bf16[128,512]{1,0:T(8,128)(2,1)S(1)}, bf16[128,512]{1,0:T(8,128)(2,1)S(1)}, u32[]{:S(2)}, u32[]{:S(2)}) collective-permute-start(bf16[128,512]{1,0:T(8,128)(2,1)S(1)} %get-tuple-element.25), channel_id=1, source_target_pairs={{0,64},{32,96},{64,0},{96,32},{1,65},{33,97},{65,1},{97,33},{2,66}... | collective-permute-start | bytes 393224 | tf_op jit(solution)/shard_map/ppermute | solution.py:40
  21.7 0.9 copy-start
  22.6 21.7 %collective-permute-start.12 = (bf16[128,2048]{1,0:T(8,128)(2,1)S(1)}, bf16[128,2048]{1,0:T(8,128)(2,1)S(1)}, u32[]{:S(2)}, u32[]{:S(2)}) collective-permute-start(bf16[128,2048]{1,0:T(8,128)(2,1)S(1)} %stack.13.refs_0_), channel_id=1, source_target_pairs={{0,2},{2,4},{4,6},{6,0},{1,3},{3,5},{5,7},{7,1},{8,10},{10,12},{12... | collective-permute-start | bytes 1572872 | tf_op jit(solution)/shard_map/ppermute | solution.py:40
  24.2 20.6 %collective-permute-start.13 = (bf16[128,2048]{1,0:T(8,128)(2,1)S(1)}, bf16[128,2048]{1,0:T(8,128)(2,1)S(1)}, u32[]{:S(2)}, u32[]{:S(2)}) collective-permute-start(bf16[128,2048]{1,0:T(8,128)(2,1)S(1)} %stack.13.refs_0_), channel_id=1, source_target_pairs={{0,6},{2,0},{4,2},{6,4},{1,7},{3,1},{5,3},{7,5},{8,14},{10,8},{12,... | collective-permute-start | bytes 1572872 | tf_op jit(solution)/shard_map/ppermute | solution.py:40
  24.7 24.5 %collective-permute-start.14 = (bf16[128,2048]{1,0:T(8,128)(2,1)S(1)}, bf16[128,2048]{1,0:T(8,128)(2,1)S(1)}, u32[]{:S(2)}, u32[]{:S(2)}) collective-permute-start(bf16[128,2048]{1,0:T(8,128)(2,1)S(1)} %stack.13.refs_0_), channel_id=1, source_target_pairs={{0,4},{2,6},{4,0},{6,2},{1,5},{3,7},{5,1},{7,3},{8,12},{10,14},{12... | collective-permute-start | bytes 1572872 | tf_op jit(solution)/shard_map/ppermute | solution.py:40
  26.9 8.7 %collective-permute-start.3 = (bf16[4,128,256]{2,1,0:T(8,128)(2,1)S(1)}, bf16[4,128,256]{2,1,0:T(8,128)(2,1)S(1)}, u32[]{:S(2)}, u32[]{:S(2)}) collective-permute-start(bf16[4,128,256]{2,1,0:T(8,128)(2,1)S(1)} %all-to-all-done.refs_4_._), channel_id=1, source_target_pairs={{0,8},{8,16},{16,24},{24,0},{1,9},{9,17},{17,25},{25,1},{2,10},{10... | collective-permute-start | bytes 786440 | tf_op jit(solution)/shard_map/ppermute | solution.py:40
  26.9 5.5 %collective-permute-start.2 = (bf16[128,512]{1,0:T(8,128)(2,1)S(1)}, bf16[128,512]{1,0:T(8,128)(2,1)S(1)}, u32[]{:S(2)}, u32[]{:S(2)}) collective-permute-start(bf16[128,512]{1,0:T(8,128)(2,1)S(1)} %get-tuple-element.26), channel_id=1, source_target_pairs={{0,96},{32,0},{64,32},{96,64},{1,97},{33,1},{65,33},{97,65},{2,98}... | collective-permute-start | bytes 393224 | tf_op jit(solution)/shard_map/ppermute | solution.py:40
  32.4 11.9 %collective-permute-start.4 = (bf16[4,128,256]{2,1,0:T(8,128)(2,1)S(1)}, bf16[4,128,256]{2,1,0:T(8,128)(2,1)S(1)}, u32[]{:S(2)}, u32[]{:S(2)}) collective-permute-start(bf16[4,128,256]{2,1,0:T(8,128)(2,1)S(1)} %all-to-all-done.refs_4_._), channel_id=1, source_target_pairs={{0,24},{8,0},{16,8},{24,16},{1,25},{9,1},{17,9},{25,17},{2,26},{10... | collective-permute-start | bytes 786440 | tf_op jit(solution)/shard_map/ppermute | solution.py:40
  35.6 13.7 %collective-permute-start.5 = (bf16[4,128,256]{2,1,0:T(8,128)(2,1)S(1)}, bf16[4,128,256]{2,1,0:T(8,128)(2,1)S(1)}, u32[]{:S(2)}, u32[]{:S(2)}) collective-permute-start(bf16[4,128,256]{2,1,0:T(8,128)(2,1)S(1)} %all-to-all-done.refs_4_._), channel_id=1, source_target_pairs={{0,16},{8,24},{16,0},{24,8},{1,17},{9,25},{17,1},{25,9},{2,18},{10... | collective-permute-start | bytes 786440 | tf_op jit(solution)/shard_map/ppermute | solution.py:40
  44.3 11.2 %collective-permute-start.15 = (bf16[128,2048]{1,0:T(8,128)(2,1)S(1)}, bf16[128,2048]{1,0:T(8,128)(2,1)S(1)}, u32[]{:S(2)}, u32[]{:S(2)}) collective-permute-start(bf16[128,2048]{1,0:T(8,128)(2,1)S(1)} %stack.13.refs_0_), channel_id=1, source_target_pairs={{0,1},{1,0},{2,3},{3,2},{4,5},{5,4},{6,7},{7,6},{8,9},{9,8},{10,11... | collective-permute-start | bytes 1572872 | tf_op jit(solution)/shard_map/ppermute | solution.py:346
  44.3 25.9 %collective-permute-start.16 = (bf16[128,2048]{1,0:T(8,128)(2,1)S(1)}, bf16[128,2048]{1,0:T(8,128)(2,1)S(1)}, u32[]{:S(2)}, u32[]{:S(2)}) collective-permute-start(bf16[128,2048]{1,0:T(8,128)(2,1)S(1)} %collective-permute-done.12.refs_1_), channel_id=1, source_target_pairs={{0,1},{1,0},{2,3},{3,2},{4,5},{5,4},{6,7},{7,6},{8,9},{9,8},{10,11... | collective-permute-start | bytes 1572872 | tf_op jit(solution)/shard_map/ppermute | solution.py:346
  44.9 26.0 %collective-permute-start.17 = (bf16[128,2048]{1,0:T(8,128)(2,1)S(1)}, bf16[128,2048]{1,0:T(8,128)(2,1)S(1)}, u32[]{:S(2)}, u32[]{:S(2)}) collective-permute-start(bf16[128,2048]{1,0:T(8,128)(2,1)S(1)} %collective-permute-done.13.refs_2_), channel_id=1, source_target_pairs={{0,1},{1,0},{2,3},{3,2},{4,5},{5,4},{6,7},{7,6},{8,9},{9,8},{10,11... | collective-permute-start | bytes 1572872 | tf_op jit(solution)/shard_map/ppermute | solution.py:346
  49.3 24.3 %collective-permute-start.18 = (bf16[128,2048]{1,0:T(8,128)(2,1)S(1)}, bf16[128,2048]{1,0:T(8,128)(2,1)S(1)}, u32[]{:S(2)}, u32[]{:S(2)}) collective-permute-start(bf16[128,2048]{1,0:T(8,128)(2,1)S(1)} %collective-permute-done.14.refs_3_), channel_id=1, source_target_pairs={{0,1},{1,0},{2,3},{3,2},{4,5},{5,4},{6,7},{7,6},{8,9},{9,8},{10,11... | collective-permute-start | bytes 1572872 | tf_op jit(solution)/shard_map/ppermute | solution.py:346
  54.0 10.0 %collective-permute-start.22 = (bf16[256,512]{1,0:T(8,128)(2,1)S(1)}, bf16[256,512]{1,0:T(8,128)(2,1)S(1)}, u32[]{:S(2)}, u32[]{:S(2)}) collective-permute-start(bf16[256,512]{1,0:T(8,128)(2,1)S(1)} %get-tuple-element.34.x0), channel_id=1, source_target_pairs={{0,32},{32,64},{64,96},{96,0},{1,33},{33,65},{65,97},{97,1},{2,34}... | collective-permute-start | bytes 786440 | tf_op jit(solution)/shard_map/ppermute | solution.py:40
  55.5 18.9 %collective-permute-start.23 = (bf16[256,512]{1,0:T(8,128)(2,1)S(1)}, bf16[256,512]{1,0:T(8,128)(2,1)S(1)}, u32[]{:S(2)}, u32[]{:S(2)}) collective-permute-start(bf16[256,512]{1,0:T(8,128)(2,1)S(1)} %get-tuple-element.34.x0), channel_id=1, source_target_pairs={{0,96},{32,0},{64,32},{96,64},{1,97},{33,1},{65,33},{97,65},{2,98}... | collective-permute-start | bytes 786440 | tf_op jit(solution)/shard_map/ppermute | solution.py:40
  64.0 10.4 %collective-permute-start.24 = (bf16[256,512]{1,0:T(8,128)(2,1)S(1)}, bf16[256,512]{1,0:T(8,128)(2,1)S(1)}, u32[]{:S(2)}, u32[]{:S(2)}) collective-permute-start(bf16[256,512]{1,0:T(8,128)(2,1)S(1)} %get-tuple-element.34.x0), channel_id=1, source_target_pairs={{0,64},{32,96},{64,0},{96,32},{1,65},{33,97},{65,1},{97,33},{2,66}... | collective-permute-start | bytes 786440 | tf_op jit(solution)/shard_map/ppermute | solution.py:40
  70.2 15.9 %collective-permute-start.6 = (bf16[256,512]{1,0:T(8,128)(2,1)S(1)}, bf16[256,512]{1,0:T(8,128)(2,1)S(1)}, u32[]{:S(2)}, u32[]{:S(2)}) collective-permute-start(bf16[256,512]{1,0:T(8,128)(2,1)S(1)} %attend.3._.x0), channel_id=1, source_target_pairs={{0,32},{32,64},{64,96},{96,0},{1,33},{33,65},{65,97},{97,1},{2,34}... | collective-permute-start | bytes 786440 | tf_op jit(solution)/shard_map/ppermute | solution.py:40
  70.9 16.9 %collective-permute-start.7 = (bf16[256,512]{1,0:T(8,128)(2,1)S(1)}, bf16[256,512]{1,0:T(8,128)(2,1)S(1)}, u32[]{:S(2)}, u32[]{:S(2)}) collective-permute-start(bf16[256,512]{1,0:T(8,128)(2,1)S(1)} %attend.3._.x0), channel_id=1, source_target_pairs={{0,96},{32,0},{64,32},{96,64},{1,97},{33,1},{65,33},{97,65},{2,98}... | collective-permute-start | bytes 786440 | tf_op jit(solution)/shard_map/ppermute | solution.py:40
  73.6 14.2 %collective-permute-start.8 = (bf16[256,512]{1,0:T(8,128)(2,1)S(1)}, bf16[256,512]{1,0:T(8,128)(2,1)S(1)}, u32[]{:S(2)}, u32[]{:S(2)}) collective-permute-start(bf16[256,512]{1,0:T(8,128)(2,1)S(1)} %attend.3._.x0), channel_id=1, source_target_pairs={{0,64},{32,96},{64,0},{96,32},{1,65},{33,97},{65,1},{97,33},{2,66}... | collective-permute-start | bytes 786440 | tf_op jit(solution)/shard_map/ppermute | solution.py:40
  75.7 18.7 %collective-permute-start.25 = (bf16[64,1024]{1,0:T(8,128)(2,1)S(1)}, bf16[64,1024]{1,0:T(8,128)(2,1)S(1)}, u32[]{:S(2)}, u32[]{:S(2)}) collective-permute-start(bf16[64,1024]{1,0:T(8,128)(2,1)S(1)} %get-tuple-element.36), channel_id=1, source_target_pairs={{0,32},{32,64},{64,96},{96,0},{1,33},{33,65},{65,97},{97,1},{2,34}... | collective-permute-start | bytes 393224 | tf_op jit(solution)/shard_map/ppermute | solution.py:40
  76.2 18.2 %collective-permute-start.26 = (bf16[64,1024]{1,0:T(8,128)(2,1)S(1)}, bf16[64,1024]{1,0:T(8,128)(2,1)S(1)}, u32[]{:S(2)}, u32[]{:S(2)}) collective-permute-start(bf16[64,1024]{1,0:T(8,128)(2,1)S(1)} %get-tuple-element.37), channel_id=1, source_target_pairs={{0,64},{32,96},{64,0},{96,32},{1,65},{33,97},{65,1},{97,33},{2,66}... | collective-permute-start | bytes 393224 | tf_op jit(solution)/shard_map/ppermute | solution.py:40
  86.1 8.3 %collective-permute-start.27 = (bf16[64,1024]{1,0:T(8,128)(2,1)S(1)}, bf16[64,1024]{1,0:T(8,128)(2,1)S(1)}, u32[]{:S(2)}, u32[]{:S(2)}) collective-permute-start(bf16[64,1024]{1,0:T(8,128)(2,1)S(1)} %get-tuple-element.38), channel_id=1, source_target_pairs={{0,96},{32,0},{64,32},{96,64},{1,97},{33,1},{65,33},{97,65},{2,98}... | collective-permute-start | bytes 393224 | tf_op jit(solution)/shard_map/ppermute | solution.py:40
  89.1 6.8 %collective-permute-start.19 = (bf16[64,1024]{1,0:T(8,128)(2,1)S(1)}, bf16[64,1024]{1,0:T(8,128)(2,1)S(1)}, u32[]{:S(2)}, u32[]{:S(2)}) collective-permute-start(bf16[64,1024]{1,0:T(8,128)(2,1)S(1)} %get-tuple-element.31), channel_id=1, source_target_pairs={{0,32},{32,64},{64,96},{96,0},{1,33},{33,65},{65,97},{97,1},{2,34}... | collective-permute-start | bytes 393224 | tf_op jit(solution)/shard_map/ppermute | solution.py:40
  89.6 9.2 %collective-permute-start.20 = (bf16[64,1024]{1,0:T(8,128)(2,1)S(1)}, bf16[64,1024]{1,0:T(8,128)(2,1)S(1)}, u32[]{:S(2)}, u32[]{:S(2)}) collective-permute-start(bf16[64,1024]{1,0:T(8,128)(2,1)S(1)} %get-tuple-element.32), channel_id=1, source_target_pairs={{0,64},{32,96},{64,0},{96,32},{1,65},{33,97},{65,1},{97,33},{2,66}... | collective-permute-start | bytes 393224 | tf_op jit(solution)/shard_map/ppermute | solution.py:40
  94.4 5.0 %collective-permute-start.21 = (bf16[64,1024]{1,0:T(8,128)(2,1)S(1)}, bf16[64,1024]{1,0:T(8,128)(2,1)S(1)}, u32[]{:S(2)}, u32[]{:S(2)}) collective-permute-start(bf16[64,1024]{1,0:T(8,128)(2,1)S(1)} %get-tuple-element.33), channel_id=1, source_target_pairs={{0,96},{32,0},{64,32},{96,64},{1,97},{33,1},{65,33},{97,65},{2,98}... | collective-permute-start | bytes 393224 | tf_op jit(solution)/shard_map/ppermute | solution.py:40
